TPU v7x, 256 devices: a whole 4x4x8 slice. The times are simulated.
256 devices in a mesh: sp: 16 (over y, x), tp: 16 (over z, core).
Axes of the slice: x: 4, y: 4, z: 8, core: 2. Of those that a mesh axis runs over, the one named last changes fastest.
Arguments:
- queries: bfloat16 [16384, 1536], P('sp', 'tp'), may hold values from -34 to 34
- latent: bfloat16 [16384, 512], P('sp'), may hold values from -6 to 6
- rot_key: bfloat16 [16384, 32], P('sp'), may hold values from -34 to 34
- latent_gain: float32 [512], replicated, may hold values from 0.1 to 1.9
- key_up: bfloat16 [512, 1024], P(None, 'tp'), may hold values from -0.25 to 0.25
- value_up: bfloat16 [512, 1024], P(None, 'tp'), may hold values from -0.70710678 to 0.70710678
- query_gain: float32 [96], replicated, may hold values from 0.5 to 6
- key_gain: float32 [96], replicated, may hold values from 0.5 to 6
- out_gain: float32 [1024], replicated, may hold values from 0.1 to 1.9
- out_weight: bfloat16 [1024, 2048], replicated, may hold values from -0.1875 to 0.1875
- residual: bfloat16 [16384, 2048], P(('sp', 'tp')), may hold values from -6 to 6
- ffn_gain: float32 [2048], replicated, may hold values from 0.1 to 1.9
- routes: int32 [16384, 2], P(('sp', 'tp')), may hold values from 0 to 15, all different within a row; in each aligned block of 64 rows (0 to 63, 64 to 127, ...) at most 9 rows name the same one
- route_weights: float32 [16384, 2], P(('sp', 'tp')), may hold values from 0.2 to 1
- expert_gate: bfloat16 [16, 2048, 2048], P('sp', None, 'tp'), may hold values from -0.125 to 0.125
- expert_up: bfloat16 [16, 2048, 2048], P('sp', None, 'tp'), may hold values from -0.125 to 0.125
- expert_down: bfloat16 [16, 2048, 2048], P('sp', 'tp'), may hold values from -0.125 to 0.125
Outputs:
- layer_out: bfloat16 [16384, 2048], P(('sp', 'tp'))
Inputs may be any that keep to these rules, and one draw needn't show every extreme that they name: `routes`: the 2 experts of a token differ. Among the 64 rows of one device each expert is named by at most 9 rows, a bound that some block reaches.
All inputs are finite; a program needn't handle non-finite values.
Results may differ from a plain program's by a relative error of at most 0.02.
The roundings to bfloat16 on the way count: a program that leaves them out, or rounds other values in their place, can miss the bound.
Values may be sent and summed in bfloat16 or wider, within the bound.
No kernel may reach another device: no remote copies, remote signals or barrier semaphores. Data moves between devices by JAX's collectives and lax.ppermute only.
A program may use at most 128 MiB of HBM per device.

v0:
```python
import jax
import jax.numpy as jnp
from jax import lax
from jax.experimental import pallas as pl
from jax.experimental.pallas import tpu as pltpu
from jax.sharding import PartitionSpec as P


D = 2048
NOPE = 64
ROPE = 32
VH = 64
QK = 96
CORES = 2
LANES = 128
TILE = 8
SIDE = 4
LOG2E = 1.4426950408889634
LOW = -1e30


epsilon = 1e-06
rope_base = 10000.0


def rms_scale(values):
    return lax.rsqrt(jnp.mean(values * values, axis=-1, keepdims=True) + epsilon)


def head_prepare(raw, gain_vec, cosine, sine_val):
    scale = lax.rsqrt(jnp.mean(raw * raw, axis=0, keepdims=True) + epsilon)
    normed = raw * scale * gain_vec[:, None]
    first = normed[NOPE : NOPE + ROPE // 2]
    second = normed[NOPE + ROPE // 2 :]
    return jnp.concatenate(
        [normed[:NOPE], first * cosine - second * sine_val, second * cosine + first * sine_val],
        axis=0,
    ).astype(jnp.bfloat16)


def attend_kernel(qs_ref, ks_ref, *refs, tq, tk, kb, parts):
    q_in, kv_in = refs[:parts], refs[parts : 2 * parts]
    out_ref = refs[2 * parts]
    q_buf, kv_buf, k_nat, v_aug, acc, peak, sems = refs[2 * parts + 1 :]
    span = kv_buf.shape[2]
    copies = []
    for i in range(parts):
        for j, (src, dst) in enumerate(((kv_in[i], kv_buf.at[i]), (q_in[i], q_buf.at[i]))):
            copy = pltpu.make_async_copy(src, dst, sems.at[2 * i + j])
            copy.start()
            copies.append(copy)
    for i in range(parts):
        copies[2 * i].wait()
        k_nat[pl.ds(i * span, span), :] = kv_buf[i, :QK, :].T
        for j in range(span // tk):
            piece = i * (span // tk) + j
            v_aug[piece, :VH, :] = kv_buf[i, QK:, j * tk : (j + 1) * tk]
            v_aug[piece, VH:, :] = jnp.ones((16, tk), jnp.bfloat16)
    for i in range(parts):
        copies[2 * i + 1].wait()

    scale = LOG2E * QK ** (-0.5)
    per_q = span // tq
    per_k = span // tk

    def q_tile(t, carry):
        i, h = t // per_q, t % per_q
        q_start = qs_ref[t]
        q = q_buf[i, :, pl.ds(pl.multiple_of(h * tq, tq), tq)]
        acc[...] = jnp.zeros_like(acc)
        peak[...] = jnp.full_like(peak, LOW)

        def k_tile(u, c):
            k_start = ks_ref[u // per_k] + (u % per_k) * tk

            def score(r, masked):
                keys = k_nat[pl.ds(pl.multiple_of(u * tk + r * kb, kb), kb), :]
                s = jnp.dot(keys, q, preferred_element_type=jnp.float32)
                if masked:
                    kpos = k_start + r * kb + lax.broadcasted_iota(jnp.int32, s.shape, 0)
                    qpos = q_start + lax.broadcasted_iota(jnp.int32, s.shape, 1)
                    s = jnp.where(kpos <= qpos, s, LOW)
                return s

            def update(masked):
                old, total = peak[0:1, :], acc[...]
                ahead = score(0, masked)
                for r in range(tk // kb):
                    s = ahead
                    if (r + 1) * kb < tk:
                        ahead = score(r + 1, masked)
                    new = jnp.maximum(old, jnp.max(s, axis=0, keepdims=True))
                    e = jnp.exp2((s - new) * scale).astype(jnp.bfloat16)
                    part = jnp.dot(
                        v_aug[u, :, r * kb : (r + 1) * kb], e, preferred_element_type=jnp.float32
                    )
                    total = total * jnp.exp2((old - new) * scale) + part
                    old = new
                acc[...] = total
                peak[...] = jnp.broadcast_to(old, peak.shape)

            @pl.when(k_start + tk - 1 <= q_start)
            def _():
                update(False)

            @pl.when((k_start + tk - 1 > q_start) & (k_start <= q_start + tq - 1))
            def _():
                update(True)

            return c

        lax.fori_loop(0, parts * per_k, k_tile, 0)
        total = acc[VH : VH + 1, :]
        live = total > 0.0
        safe = jnp.where(live, total, 1.0)
        lse = jnp.where(live, peak[0:1, :] * scale + jnp.log2(safe), LOW)
        hi = lse.astype(jnp.bfloat16)
        mid = (lse - hi.astype(jnp.float32)).astype(jnp.bfloat16)
        lo = (lse - hi.astype(jnp.float32) - mid.astype(jnp.float32)).astype(jnp.bfloat16)
        row = lax.broadcasted_iota(jnp.int32, (16, tq), 0)
        stats = jnp.where(
            row == 0,
            hi.astype(jnp.float32),
            jnp.where(row == 1, mid.astype(jnp.float32), jnp.where(row == 2, lo.astype(jnp.float32), 0.0)),
        )
        cols = pl.ds(pl.multiple_of(h * tq, tq), tq)
        out_ref[i, :VH, cols] = (acc[:VH, :] / safe).astype(jnp.bfloat16)
        out_ref[i, VH:, cols] = stats.astype(jnp.bfloat16)
        return carry

    lax.fori_loop(0, parts * per_q, q_tile, 0)


def attend(q_parts, kv_parts, q_starts, k_starts, tq=512, tk=1024, kb=512):
    parts = len(q_parts)
    span = q_parts[0].shape[1]
    hbm = pl.BlockSpec(memory_space=pltpu.HBM)
    smem = pl.BlockSpec(memory_space=pltpu.SMEM)

    def kernel(*refs):
        attend_kernel(*refs, tq=tq, tk=tk, kb=kb, parts=parts)

    work = parts * parts * span * span // 2
    return pl.pallas_call(
        kernel,
        out_shape=jax.ShapeDtypeStruct((parts, VH + 16, span), jnp.bfloat16),
        in_specs=[smem, smem] + [hbm] * (2 * parts),
        out_specs=pl.BlockSpec(memory_space=pltpu.VMEM),
        scratch_shapes=[
            pltpu.VMEM((parts, QK, span), jnp.bfloat16),
            pltpu.VMEM((parts, QK + VH, span), jnp.bfloat16),
            pltpu.VMEM((parts * span, QK), jnp.bfloat16),
            pltpu.VMEM((parts * span // tk, VH + 16, tk), jnp.bfloat16),
            pltpu.VMEM((VH + 16, tq), jnp.float32),
            pltpu.VMEM((8, tq), jnp.float32),
            pltpu.SemaphoreType.DMA((2 * parts,)),
        ],
        compiler_params=pltpu.CompilerParams(vmem_limit_bytes=60 * 1024 * 1024),
        cost_estimate=pl.CostEstimate(
            flops=2 * work * (QK + VH), bytes_accessed=3 * 1024 * 1024, transcendentals=work
        ),
        name="attend",
    )(q_starts, k_starts, *q_parts, *kv_parts)


def expert_group(rows, w_buf, slots):
    width = w_buf.shape[2]
    weights = jnp.concatenate(
        [w_buf[s, :D, :] for s in slots] + [w_buf[s, D : 2 * D, :] for s in slots], axis=1
    )
    both = jnp.dot(rows, weights, preferred_element_type=jnp.float32)
    half = both.shape[1] // 2
    gate, up = both[:, :half], both[:, half:]
    hidden = (gate / (1.0 + jnp.exp(-gate)) * up).astype(jnp.bfloat16)
    down = jnp.concatenate(
        [
            jnp.concatenate(
                [w_buf[s, 2 * D + j * width : 2 * D + (j + 1) * width, :] for s in slots], axis=0
            )
            for j in range(D // LANES)
        ],
        axis=1,
    )
    return jnp.dot(hidden, down, preferred_element_type=jnp.float32)


def expert_kernel(*refs, places, pairs, adds, ends):
    total = len(places)
    x_ref, y_ref = refs[:2]
    before, refs = refs[2 : 2 + adds], refs[2 + adds :]
    w_refs, refs = refs[:total], refs[total:]
    outs, (acc, w_buf, sems) = refs[:-3], refs[-3:]
    copies = [
        pltpu.make_async_copy(w_refs[i], w_buf.at[s, pl.ds(first, size)], sems.at[i])
        for i, (s, first, size) in enumerate(places)
    ]
    for copy in copies:
        copy.start()
    rows = jnp.concatenate([x_ref[...], y_ref[...]], axis=0)
    slices = w_buf.shape[0]
    first = 0
    while first < slices:
        slots = list(range(first, min(slices, first + (pairs if slices % pairs == 0 or first else 1))))
        for copy, place in zip(copies, places):
            if place[0] in slots:
                copy.wait()
        part = expert_group(rows, w_buf, slots)
        if first:
            part = acc[...] + part
        elif adds:
            part = before[0][...] + part
        acc[...] = part
        first = slots[-1] + 1
    if ends:
        count = x_ref.shape[0]
        outs[0][...] = acc[:count, :].astype(jnp.bfloat16)
        outs[1][...] = acc[count:, :].astype(jnp.bfloat16)
    else:
        outs[0][...] = acc[...]


def expert_ffn(rows, others, before, pieces, places, ends):
    count = rows.shape[0]
    slices, depth, width = 1 + max(p[0] for p in places), 3 * D, LANES
    vmem = pl.BlockSpec(memory_space=pltpu.VMEM)
    hbm = pl.BlockSpec(memory_space=pltpu.HBM)
    if ends:
        outs = [jax.ShapeDtypeStruct((count, D), jnp.bfloat16)] * 2
    else:
        outs = [jax.ShapeDtypeStruct((2 * count, D), jnp.float32)]

    def kernel(*refs):
        expert_kernel(*refs, places=places, pairs=2, adds=len(before), ends=ends)

    return pl.pallas_call(
        kernel,
        out_shape=outs,
        in_specs=[vmem, vmem] + [vmem] * len(before) + [hbm] * len(pieces),
        out_specs=[vmem] * len(outs),
        scratch_shapes=[
            pltpu.VMEM((2 * count, D), jnp.float32),
            pltpu.VMEM((slices, depth, width), jnp.bfloat16),
            pltpu.SemaphoreType.DMA((len(pieces),)),
        ],
        compiler_params=pltpu.CompilerParams(vmem_limit_bytes=58 * 1024 * 1024),
        cost_estimate=pl.CostEstimate(
            flops=12 * count * D * slices * width,
            bytes_accessed=6 * D * slices * width,
            transcendentals=2 * count * slices * width,
        ),
    )(rows, others, *before, *pieces)


def to_wire(rows, peers):
    tiles = D // LANES
    main = rows[: peers * TILE].reshape(peers, TILE, tiles, LANES)
    main = main.transpose(0, 2, 1, 3).reshape(peers, tiles * TILE, LANES)
    return jnp.concatenate([main, rows[peers * TILE :].reshape(peers, tiles, LANES)], axis=1)


def from_wire(wire):
    peers = wire.shape[0]
    tiles = D // LANES
    main = wire[:, : tiles * TILE].reshape(peers, tiles, TILE, LANES)
    main = main.transpose(0, 2, 1, 3).reshape(peers * TILE, D)
    return jnp.concatenate([main, wire[:, tiles * TILE :].reshape(peers, D)], axis=0)


def slot_targets(route_rows, expert_total):
    flat_routes = route_rows.reshape(-1)
    one_hot = (flat_routes[:, None] == jnp.arange(expert_total, dtype=jnp.int32)[None, :]).astype(
        jnp.int32
    )
    earlier = jnp.cumsum(one_hot, axis=0) - one_hot
    rank_in = jnp.sum(earlier * one_hot, axis=1)
    slots = jnp.where(
        rank_in < TILE, flat_routes * TILE + rank_in, expert_total * TILE + flat_routes
    )
    return slots.reshape(route_rows.shape)


def select_matrix(targets, slot_total):
    hits = targets[:, :, None] == jnp.arange(slot_total, dtype=jnp.int32)[None, None, :]
    return jnp.sum(hits.astype(jnp.bfloat16), axis=1)


def row_shift(value, k):
    pairs = [
        (y * SIDE + x, y * SIDE + (x + k) % SIDE) for y in range(SIDE) for x in range(SIDE)
    ]
    return lax.ppermute(value, "sp", pairs)


def column_shift(value, k):
    pairs = [
        (y * SIDE + x, ((y + k) % SIDE) * SIDE + x) for y in range(SIDE) for x in range(SIDE)
    ]
    return lax.ppermute(value, "sp", pairs)


def row_swap(value):
    pairs = [
        (y * SIDE + x, (SIDE - 1 - y) * SIDE + x) for y in range(SIDE) for x in range(SIDE)
    ]
    return lax.ppermute(value, "sp", pairs)


def expert_exchange(wire):
    return lax.all_to_all(wire, "sp", split_axis=0, concat_axis=0, tiled=True)


def z_shift(value, k):
    count = lax.axis_size("tp")
    return lax.ppermute(value, "tp", [(t, (t + CORES * k) % count) for t in range(count)])


def core_swap(value):
    pairs = [(t, t ^ 1) for t in range(lax.axis_size("tp"))]
    return lax.ppermute(value, "tp", pairs)


def shards(
    queries,
    latent,
    rot_key,
    latent_gain,
    key_up,
    value_up,
    query_gain,
    key_gain,
    out_gain,
    out_weight,
    residual,
    ffn_gain,
    routes,
    route_weights,
    expert_gate,
    expert_up,
    expert_down,
):
    shard_len = queries.shape[0]
    half_len = shard_len // 2
    sp_count = lax.axis_size("sp")
    me = lax.axis_index("sp")
    my_y, my_x = me // SIDE, me % SIDE

    gate, up, down = expert_gate[0], expert_up[0], expert_down[0]
    down = down.reshape(down.shape[0], D // LANES, LANES).transpose(1, 0, 2).reshape(-1, LANES)
    halves = [
        jnp.concatenate([gate, up[: D // 2]], axis=0),
        jnp.concatenate([up[D // 2 :], down], axis=0),
    ]
    ahead, behind = [[half] for half in halves], [[half] for half in halves]

    def ring_step(h, n):
        front, back = ahead[h][-1], behind[h][-1]
        if n < 4 or h == 0:
            ahead[h].append(z_shift(front, 1))
        if n < 4 or h == 1:
            behind[h].append(z_shift(back, -1))

    for n in (1, 2, 3, 4):
        for h in (0, 1):
            ring_step(h, n)

    positions = me * shard_len + jnp.arange(shard_len, dtype=jnp.int32)
    inverse = rope_base ** (-jnp.arange(0, ROPE, 2, dtype=jnp.float32) / ROPE)
    angles = positions.astype(jnp.float32)[None, :] * inverse[:, None]
    cosine, sine_val = jnp.cos(angles), jnp.sin(angles)

    query_rows = head_prepare(queries.astype(jnp.float32).T, query_gain, cosine, sine_val)
    swapped = row_swap(query_rows[:, half_len:])
    q_set = jnp.concatenate([query_rows[:, :half_len], swapped], axis=1)

    lat_f32 = latent.astype(jnp.float32)
    normed_latent = (lat_f32 * rms_scale(lat_f32) * latent_gain).astype(jnp.bfloat16)
    both_up = jnp.concatenate([key_up, value_up], axis=1)
    lifted = lax.dot_general(
        both_up, normed_latent, (((0,), (1,)), ((), ())), preferred_element_type=jnp.float32
    ).astype(jnp.bfloat16)
    raw_keys = jnp.concatenate(
        [lifted[:NOPE].astype(jnp.float32), rot_key.astype(jnp.float32).T], axis=0
    )
    bundle = jnp.concatenate(
        [head_prepare(raw_keys, key_gain, cosine, sine_val), lifted[NOPE:]], axis=0
    )

    shifts = range(SIDE)
    kv_parts = [bundle] + [column_shift(bundle, k) for k in shifts[1:]]
    q_parts = [q_set] + [row_shift(q_set, k) for k in shifts[1:]]
    k_starts = jnp.stack([((my_y - k) % SIDE * SIDE + my_x) * shard_len for k in shifts])
    q_cols = [(my_x - k) % SIDE for k in shifts]
    q_starts = jnp.stack(
        sum(
            [
                [
                    (my_y * SIDE + c) * shard_len,
                    ((SIDE - 1 - my_y) * SIDE + c) * shard_len + half_len,
                ]
                for c in q_cols
            ],
            [],
        )
    )
    partial = attend(q_parts, kv_parts, q_starts.astype(jnp.int32), k_starts.astype(jnp.int32))
    pieces = [partial[0]] + [row_shift(partial[k], -k) for k in shifts[1:]]
    levels = [jnp.sum(p[VH : VH + 3].astype(jnp.float32), axis=0, keepdims=True) for p in pieces]
    top = levels[0]
    for level in levels[1:]:
        top = jnp.maximum(top, level)
    factors = [jnp.exp2(level - top) for level in levels]
    merged = sum(w * p[:VH].astype(jnp.float32) for w, p in zip(factors, pieces)) / sum(factors)
    merged = merged.astype(jnp.bfloat16)
    back = row_swap(merged[:, half_len:])
    attended = jnp.concatenate([merged[:, :half_len], back], axis=1)

    token_rows = lax.all_to_all(attended.T, "tp", split_axis=0, concat_axis=1, tiled=True)
    token_rows = token_rows.astype(jnp.float32)
    normed_rows = (token_rows * rms_scale(token_rows) * out_gain).astype(jnp.bfloat16)
    mixed = jnp.dot(normed_rows, out_weight, preferred_element_type=jnp.float32)
    middle = residual.astype(jnp.float32) + mixed
    ffn_input = (middle * rms_scale(middle) * ffn_gain).astype(jnp.bfloat16)
    slot_total = sp_count * (TILE + 1)
    targets = slot_targets(routes, sp_count)
    chooser = select_matrix(targets, slot_total)
    outbound = jnp.einsum(
        "ts,td->sd", chooser, ffn_input, preferred_element_type=jnp.float32
    ).astype(jnp.bfloat16)
    arrived = expert_exchange(to_wire(outbound, sp_count))
    my_rows = from_wire(arrived)
    their_rows = core_swap(my_rows)
    weight_pieces, places = [], []
    for h, half in enumerate(halves):
        size = half.shape[0]
        start = h * size
        for n in range(4):
            for way, ring in ((0, ahead[h]), (1, behind[h])):
                if n == 0 and way == 1:
                    continue
                weight_pieces.append(ring[n])
                places.append((2 * n - 1 + way if n else 0, start, size))
    first_sum = expert_ffn(my_rows, their_rows, [], weight_pieces, places, False)
    last_pieces = [ahead[0][4], behind[1][4]]
    size = halves[0].shape[0]
    last_places = [(0, 0, size), (0, size, size)]
    own_sum, other_sum = expert_ffn(my_rows, their_rows, first_sum, last_pieces, last_places, True)
    served = (
        own_sum.astype(jnp.float32) + core_swap(other_sum).astype(jnp.float32)
    ).astype(jnp.bfloat16)
    returned_rows = from_wire(expert_exchange(to_wire(served, sp_count)))
    hits = targets[:, :, None] == jnp.arange(slot_total, dtype=jnp.int32)[None, None, :]
    shares = jnp.sum(jnp.where(hits, route_weights[:, :, None], 0.0), axis=1)
    moe_sum = jnp.dot(
        shares,
        returned_rows.astype(jnp.float32),
        precision=lax.Precision.HIGHEST,
        preferred_element_type=jnp.float32,
    )
    return (middle + moe_sum).astype(jnp.bfloat16)


def solution(mesh):
    return jax.shard_map(
        shards,
        mesh=mesh,
        in_specs=(
            P("sp", "tp"),
            P("sp", None),
            P("sp", None),
            P(),
            P(None, "tp"),
            P(None, "tp"),
            P(),
            P(),
            P(),
            P(),
            P(("sp", "tp"), None),
            P(),
            P(("sp", "tp"), None),
            P(("sp", "tp"), None),
            P("sp", None, "tp"),
            P("sp", None, "tp"),
            P("sp", "tp", None),
        ),
        out_specs=P(("sp", "tp"), None),
        check_vma=False,
    )
```

profile of v0, /device:TPU:1, one launch (start us, length us, event | category | flops | bytes accessed | tf_op | source)
XLA Modules:
  0.0 219.0 jit_solution(7911820966873936978)
XLA Ops:
  0.0 1.5 fusion.1
  1.6 2.0 convolution_convert_fusion.1
  4.0 0.3 fusion.42
  4.4 2.2 %collective-permute-start.4 = (bf16[160,1024]{1,0:T(8,128)(2,1)S(1)}, bf16[160,1024]{1,0:T(8,128)(2,1)S(1)}, u32[]{:S(2)}, u32[]{:S(2)}) collective-permute-start(bf16[160,1024]{1,0:T(8,128)(2,1)S(1)} %pad_maximum_fusion.5.refs_6_), channel_id=1, source_target_pairs={{0,64},{16,80},{32,96},{48,112},{64,128},{80,144},{96,160},{112,17... | collective-permute-start | bytes 983048 | tf_op jit(solution)/shard_map/ppermute | solution.py:298
  6.6 2.6 %collective-permute-start.5 = (bf16[160,1024]{1,0:T(8,128)(2,1)S(1)}, bf16[160,1024]{1,0:T(8,128)(2,1)}, u32[]{:S(2)}, u32[]{:S(2)}) collective-permute-start(bf16[160,1024]{1,0:T(8,128)(2,1)S(1)} %pad_maximum_fusion.5.refs_6_), channel_id=1, source_target_pairs={{0,128},{16,144},{32,160},{48,176},{64,192},{80,208},{96,224},{112... | collective-permute-start | bytes 983048 | tf_op jit(solution)/shard_map/ppermute | solution.py:298
  9.2 1.1 collective-permute-start.6
  10.8 14.2 %collective-permute-done = bf16[96,512]{1,0:T(8,128)(2,1)S(1)} collective-permute-done((bf16[96,512]{1,0:T(8,128)(2,1)S(1)}, bf16[96,512]{1,0:T(8,128)(2,1)S(1)}, u32[]{:S(2)}, u32[]{:S(2)}) %collective-permute-start) | collective-permute-done | bytes 98336 | tf_op jit(solution)/shard_map/ppermute | solution.py:305
  25.0 1.3 collective-permute-start.1
  26.4 2.5 %collective-permute-start.2 = (bf16[96,1024]{1,0:T(8,128)(2,1)S(1)}, bf16[96,1024]{1,0:T(8,128)(2,1)}, u32[]{:S(2)}, u32[]{:S(2)}) collective-permute-start(bf16[96,1024]{1,0:T(8,128)(2,1)S(1)} %pad_maximum_fusion.7.refs_2_), channel_id=1, source_target_pairs={{0,32},{16,48},{32,0},{48,16},{64,96},{80,112},{96,64},{112,80},{1... | collective-permute-start | bytes 589832 | tf_op jit(solution)/shard_map/ppermute | solution.py:291
  28.9 3.0 %collective-permute-done.1.refs_3_ = bf16[96,1024]{1,0:T(8,128)(2,1)S(1)} collective-permute-done((bf16[96,1024]{1,0:T(8,128)(2,1)S(1)}, bf16[96,1024]{1,0:T(8,128)(2,1)S(1)}, u32[]{:S(2)}, u32[]{:S(2)}) %collective-permute-start.1) | collective-permute-done | bytes 196640 | tf_op jit(solution)/shard_map/ppermute | solution.py:291
  32.0 1.3 collective-permute-start.3
  33.6 0.1 eq.45
  33.7 0.6 stack.50.refs_0_
  34.3 0.7 pad_add_fusion.refs_1_
  35.0 2.3 %collective-permute-done.2.refs_4_ = bf16[96,1024]{1,0:T(8,128)(2,1)} collective-permute-done((bf16[96,1024]{1,0:T(8,128)(2,1)S(1)}, bf16[96,1024]{1,0:T(8,128)(2,1)}, u32[]{:S(2)}, u32[]{:S(2)}) %collective-permute-start.2) | collective-permute-done | bytes 196640 | tf_op jit(solution)/shard_map/ppermute | solution.py:291
  37.3 5.6 %collective-permute-start.19 = (bf16[3072,128]{1,0:T(8,128)(2,1)S(1)}, bf16[3072,128]{1,0:T(8,128)(2,1)S(1)}, u32[]{:S(2)}, u32[]{:S(2)}) collective-permute-start(bf16[3072,128]{1,0:T(8,128)(2,1)S(1)} %pad_maximum_fusion.1.refs_9_), channel_id=1, source_target_pairs={{0,14},{1,15},{2,0},{3,1},{4,2},{5,3},{6,4},{7,5},{8,6},{9,7},{10,... | collective-permute-start | bytes 2359304 | tf_op jit(solution)/shard_map/ppermute | solution.py:314
  43.0 0.6 copy-done.23
  43.6 22.6 %attend.1 = bf16[4,80,1024]{2,1,0:T(8,128)(2,1)} custom-call(s32[8]{0:T(128)} %stack.50.refs_0_, s32[4]{0:T(128)} %pad_add_fusion.refs_1_, bf16[96,1024]{1,0:T(8,128)(2,1)} %copy-done.16, bf16[96,1024]{1,0:T(8,128)(2,1)} %copy-done.24, bf16[96,1024]{1,0:T(8,128)(2,1)} %collective-permute-done.2.refs_4_, bf16[96,1024]{1,0:T(8,128)(2,1)} %collective-permute-done.3.refs_5_, ...), custom_call_target="tpu_custom_call" | custom-call | flops 2684354560 | bytes 3145728 | tf_op jit(solution)/shard_map/attend/pallas_call | solution.py:144
  66.2 1.1 slice_bitcast_fusion.8
  67.3 0.3 collective-permute-start.9
  67.6 0.2 reduce_window_sum.11
  67.9 0.7 convert_reduce_fusion.3
  68.6 9.2 %collective-permute-done.9 = bf16[80,1024]{1,0:T(8,128)(2,1)S(1)} collective-permute-done((bf16[80,1024]{1,0:T(8,128)(2,1)S(1)}, bf16[80,1024]{1,0:T(8,128)(2,1)S(1)}, u32[]{:S(2)}, u32[]{:S(2)}) %collective-permute-start.9) | collective-permute-done | bytes 163872 | tf_op jit(solution)/shard_map/ppermute | solution.py:291
  77.9 2.4 %collective-permute-start.13 = (bf16[3072,128]{1,0:T(8,128)(2,1)S(1)}, bf16[3072,128]{1,0:T(8,128)(2,1)}, u32[]{:S(2)}, u32[]{:S(2)}) collective-permute-start(bf16[3072,128]{1,0:T(8,128)(2,1)S(1)} %pad_maximum_fusion.refs_2_), channel_id=1, source_target_pairs={{0,14},{1,15},{2,0},{3,1},{4,2},{5,3},{6,4},{7,5},{8,6},{9,7},{10,... | collective-permute-start | bytes 2359304 | tf_op jit(solution)/shard_map/ppermute | solution.py:314
  80.3 2.3 %collective-permute-done.7 = bf16[80,1024]{1,0:T(8,128)(2,1)S(1)} collective-permute-done((bf16[80,1024]{1,0:T(8,128)(2,1)S(1)}, bf16[80,1024]{1,0:T(8,128)(2,1)S(1)}, u32[]{:S(2)}, u32[]{:S(2)}) %collective-permute-start.7) | collective-permute-done | bytes 163872 | tf_op jit(solution)/shard_map/ppermute | solution.py:291
  82.7 1.0 fusion.22
  83.7 3.9 %collective-permute-start.10 = (bf16[64,512]{1,0:T(8,128)(2,1)S(1)}, bf16[64,512]{1,0:T(8,128)(2,1)S(1)}, u32[]{:S(2)}, u32[]{:S(2)}) collective-permute-start(bf16[64,512]{1,0:T(8,128)(2,1)S(1)} %get-tuple-element.28), channel_id=1, source_target_pairs={{0,192},{16,208},{32,224},{48,240},{64,128},{80,144},{96,160},{112... | collective-permute-start | bytes 196616 | tf_op jit(solution)/shard_map/ppermute | solution.py:305
  87.6 0.2 select_reduce_fusion.1
  87.8 0.1 reduce_sum.122
  88.0 1.3 collective-permute-done.10
  89.3 0.2 copy.57
  89.5 0.9 reshape.212
  90.4 7.1 %all-to-all-start = ((bf16[16,2,2048]{2,1,0:T(2,128)(2,1)}), bf16[16,2,2048]{2,1,0:T(2,128)(2,1)S(1)}, u32[]{:S(2)}, u32[]{:S(2)}) async-start(bf16[16,2,2048]{2,1,0:T(2,128)(2,1)} %reshape.212), calls=%async_computation | async-start | bytes 262144 | tf_op jit(solution)/shard_map/all_to_all | solution.py:417
  97.6 2.6 %collective-permute-start.21 = (bf16[3072,128]{1,0:T(8,128)(2,1)S(1)}, bf16[3072,128]{1,0:T(8,128)(2,1)}, u32[]{:S(2)}, u32[]{:S(2)}) collective-permute-start(bf16[3072,128]{1,0:T(8,128)(2,1)S(1)} %collective-permute-done.19.refs_11_), channel_id=1, source_target_pairs={{0,14},{1,15},{2,0},{3,1},{4,2},{5,3},{6,4},{7,5},{8,6},{9,7},{10,... | collective-permute-start | bytes 2359304 | tf_op jit(solution)/shard_map/ppermute | solution.py:314
  100.3 6.6 %all-to-all-done = bf16[16,2,2048]{2,1,0:T(2,128)(2,1)S(1)} async-done(((bf16[16,2,2048]{2,1,0:T(2,128)(2,1)}), bf16[16,2,2048]{2,1,0:T(2,128)(2,1)S(1)}, u32[]{:S(2)}, u32[]{:S(2)}) %all-to-all-start) | async-done | bytes 131104 | tf_op jit(solution)/shard_map/all_to_all | solution.py:417
  106.8 0.2 reshape.213
  107.1 0.2 fusion.10
  107.3 0.3 copy.52
  107.6 0.2 reshape.211
  107.8 3.2 %multiply_reduce_fusion = (f32[64]{0:T(128)S(1)}, f32[64,2048]{1,0:T(8,128)S(1)}) fusion(bf16[1024,2048]{1,0:T(8,128)(2,1)} %param.26, f32[64,1024]{1,0:T(8,128)S(1)} %reshape.211, f32[1024]{0:T(1024)S(1)} %copy-done.18, f32[64]{0:T(128)S(1)} %add_rsqrt_fusion.4, bf16[64,2048]{1,0:T(8,128)(2,1)S(1)} %copy-done.14), kind=kOutput, calls=%fused_computation.29 | convolution fusion | flops 269156288 | bytes 5247488 | tf_op jit(solution)/shard_map/dot_general | solution.py:420
  111.1 0.4 convolution_convert_fusion
  111.5 0.9 pad_maximum_fusion.2
  112.4 5.3 %all-to-all-start.1 = ((bf16[16,144,128]{2,1,0:T(8,128)(2,1)}), bf16[16,144,128]{2,1,0:T(8,128)(2,1)S(1)}, u32[]{:S(2)}, u32[]{:S(2)}) async-start(bf16[16,144,128]{2,1,0:T(8,128)(2,1)} %pad_maximum_fusion.2), calls=%async_computation.1 | async-start | bytes 1179648 | tf_op jit(solution)/shard_map/all_to_all | solution.py:309
  117.8 2.7 %collective-permute-start.15 = (bf16[3072,128]{1,0:T(8,128)(2,1)}, bf16[3072,128]{1,0:T(8,128)(2,1)S(1)}, u32[]{:S(2)}, u32[]{:S(2)}) collective-permute-start(bf16[3072,128]{1,0:T(8,128)(2,1)} %collective-permute-done.13.refs_4_), channel_id=1, source_target_pairs={{0,14},{1,15},{2,0},{3,1},{4,2},{5,3},{6,4},{7,5},{8,6},{9,7},{10,... | collective-permute-start | bytes 2359304 | tf_op jit(solution)/shard_map/ppermute | solution.py:314
  120.4 10.3 %all-to-all-done.1 = bf16[16,144,128]{2,1,0:T(8,128)(2,1)S(1)} async-done(((bf16[16,144,128]{2,1,0:T(8,128)(2,1)}), bf16[16,144,128]{2,1,0:T(8,128)(2,1)S(1)}, u32[]{:S(2)}, u32[]{:S(2)}) %all-to-all-start.1) | async-done | bytes 589856 | tf_op jit(solution)/shard_map/all_to_all | solution.py:309
  130.9 1.4 collective-permute-start.16
  132.4 6.3 %collective-permute-done.20.refs_12_ = bf16[3072,128]{1,0:T(8,128)(2,1)} collective-permute-done((bf16[3072,128]{1,0:T(8,128)(2,1)}, bf16[3072,128]{1,0:T(8,128)(2,1)}, u32[]{:S(2)}, u32[]{:S(2)}) %collective-permute-start.20) | collective-permute-done | bytes 786464 | tf_op jit(solution)/shard_map/ppermute | solution.py:314
  138.7 2.7 %collective-permute-start.17 = (bf16[3072,128]{1,0:T(8,128)(2,1)S(1)}, bf16[3072,128]{1,0:T(8,128)(2,1)}, u32[]{:S(2)}, u32[]{:S(2)}) collective-permute-start(bf16[3072,128]{1,0:T(8,128)(2,1)S(1)} %collective-permute-done.15.refs_6_), channel_id=1, source_target_pairs={{0,14},{1,15},{2,0},{3,1},{4,2},{5,3},{6,4},{7,5},{8,6},{9,7},{10,... | collective-permute-start | bytes 2359304 | tf_op jit(solution)/shard_map/ppermute | solution.py:314
  141.4 1.5 collective-permute-start.11
  143.0 11.6 %collective-permute-done.23.refs_15_ = bf16[3072,128]{1,0:T(8,128)(2,1)S(1)} collective-permute-done((bf16[3072,128]{1,0:T(8,128)(2,1)}, bf16[3072,128]{1,0:T(8,128)(2,1)S(1)}, u32[]{:S(2)}, u32[]{:S(2)}) %collective-permute-start.23) | collective-permute-done | bytes 786464 | tf_op jit(solution)/shard_map/ppermute | solution.py:314
  154.5 3.3 %collective-permute-start.25 = (bf16[3072,128]{1,0:T(8,128)(2,1)S(1)}, bf16[3072,128]{1,0:T(8,128)(2,1)}, u32[]{:S(2)}, u32[]{:S(2)}) collective-permute-start(bf16[3072,128]{1,0:T(8,128)(2,1)S(1)} %collective-permute-done.23.refs_15_), channel_id=1, source_target_pairs={{0,14},{1,15},{2,0},{3,1},{4,2},{5,3},{6,4},{7,5},{8,6},{9,7},{10,... | collective-permute-start | bytes 2359304 | tf_op jit(solution)/shard_map/ppermute | solution.py:314
  157.9 14.4 %collective-permute-done.22.refs_14_ = bf16[3072,128]{1,0:T(8,128)(2,1)S(1)} collective-permute-done((bf16[3072,128]{1,0:T(8,128)(2,1)}, bf16[3072,128]{1,0:T(8,128)(2,1)S(1)}, u32[]{:S(2)}, u32[]{:S(2)}) %collective-permute-start.22) | collective-permute-done | bytes 786464 | tf_op jit(solution)/shard_map/ppermute | solution.py:314
  172.4 0.8 copy-done.8
  173.2 11.7 %shard_map.163.refs_2_ = f32[288,2048]{1,0:T(8,128)} custom-call(bf16[144,2048]{1,0:T(8,128)(2,1)} %copy-done, bf16[144,2048]{1,0:T(8,128)(2,1)} %copy-done.3, bf16[3072,128]{1,0:T(8,128)(2,1)} %copy-done.2, bf16[3072,128]{1,0:T(8,128)(2,1)} %collective-permute-done.12.refs_3_, bf16[3072,128]{1,0:T(8,128)(2,1)} %collective-permute-done.13.refs_4_, ...), custom_call_target="tpu_custom_call" | custom-call | flops 3170893824 | bytes 11010048 | tf_op jit(solution)/shard_map/pallas_call | solution.py:235
  184.9 3.2 %collective-permute-done.25.refs_4_ = bf16[3072,128]{1,0:T(8,128)(2,1)} collective-permute-done((bf16[3072,128]{1,0:T(8,128)(2,1)S(1)}, bf16[3072,128]{1,0:T(8,128)(2,1)}, u32[]{:S(2)}, u32[]{:S(2)}) %collective-permute-start.25) | collective-permute-done | bytes 786464 | tf_op jit(solution)/shard_map/ppermute | solution.py:314
  188.1 1.1 collective-permute-done.24.refs_3_
  189.3 5.8 %shard_map.164 = (bf16[144,2048]{1,0:T(8,128)(2,1)}, bf16[144,2048]{1,0:T(8,128)(2,1)}) custom-call(bf16[144,2048]{1,0:T(8,128)(2,1)} %copy-done, bf16[144,2048]{1,0:T(8,128)(2,1)} %copy-done.3, f32[288,2048]{1,0:T(8,128)} %shard_map.163.refs_2_, bf16[3072,128]{1,0:T(8,128)(2,1)} %collective-permute-done.24.refs_3_, ...), custom_call_target="tpu_custom_call" | custom-call | flops 452984832 | bytes 1572864 | tf_op jit(solution)/shard_map/pallas_call | solution.py:235
  195.1 0.6 collective-permute-start.26
  195.7 1.8 collective-permute-done.26
  197.6 1.2 add_convert_fusion
  198.9 0.9 pad_maximum_fusion.4
  199.7 6.7 %all-to-all-start.2 = ((bf16[16,144,128]{2,1,0:T(8,128)(2,1)}), bf16[16,144,128]{2,1,0:T(8,128)(2,1)S(1)}, u32[]{:S(2)}, u32[]{:S(2)}) async-start(bf16[16,144,128]{2,1,0:T(8,128)(2,1)} %pad_maximum_fusion.4), calls=%async_computation.2 | async-start | bytes 1179648 | tf_op jit(solution)/shard_map/all_to_all | solution.py:309
  206.5 11.3 %all-to-all-done.2 = bf16[16,144,128]{2,1,0:T(8,128)(2,1)S(1)} async-done(((bf16[16,144,128]{2,1,0:T(8,128)(2,1)}), bf16[16,144,128]{2,1,0:T(8,128)(2,1)S(1)}, u32[]{:S(2)}, u32[]{:S(2)}) %all-to-all-start.2) | async-done | bytes 589856 | tf_op jit(solution)/shard_map/all_to_all | solution.py:309
  217.9 1.1 fusion
  (122 shorter events, 2.3 us)
Async XLA Ops:
  1.5 2.1 copy-start.15
  1.5 2.2 copy-start.9
  1.5 2.2 %copy-start.21 = (f32[96]{0:T(128)S(1)}, f32[96]{0:T(128)}, u32[]{:S(2)}) copy-start(f32[96]{0:T(128)} %param.24) | copy-start | bytes 1156
  1.6 2.4 %copy-start.22 = (f32[96]{0:T(128)S(1)}, f32[96]{0:T(128)}, u32[]{:S(2)}) copy-start(f32[96]{0:T(128)} %param.23) | copy-start | bytes 1156
  3.9 6.6 %copy-start.11 = (bf16[1,2048,128]{2,1,0:T(8,128)(2,1)S(1)}, bf16[1,2048,128]{2,1,0:T(8,128)(2,1)}, u32[]{:S(2)}) copy-start(bf16[1,2048,128]{2,1,0:T(8,128)(2,1)} %param.32) | copy-start | bytes 1572868
  4.0 6.5 %copy-start.12 = (bf16[1,128,2048]{2,1,0:T(8,128)(2,1)S(1)}, bf16[1,128,2048]{2,1,0:T(8,128)(2,1)}, u32[]{:S(2)}) copy-start(bf16[1,128,2048]{2,1,0:T(8,128)(2,1)} %param.33) | copy-start | bytes 1572868
  4.4 6.2 %copy-start.13 = (bf16[160,1024]{1,0:T(8,128)(2,1)}, bf16[160,1024]{1,0:T(8,128)(2,1)S(1)}, u32[]{:S(2)}) copy-start(bf16[160,1024]{1,0:T(8,128)(2,1)S(1)} %pad_maximum_fusion.5.refs_6_) | copy-start | bytes 983044
  4.4 38.4 %collective-permute-start.4 = (bf16[160,1024]{1,0:T(8,128)(2,1)S(1)}, bf16[160,1024]{1,0:T(8,128)(2,1)S(1)}, u32[]{:S(2)}, u32[]{:S(2)}) collective-permute-start(bf16[160,1024]{1,0:T(8,128)(2,1)S(1)} %pad_maximum_fusion.5.refs_6_), channel_id=1, source_target_pairs={{0,64},{16,80},{32,96},{48,112},{64,128},{80,144},{96,160},{112,17... | collective-permute-start | bytes 983048 | tf_op jit(solution)/shard_map/ppermute | solution.py:298
  6.6 36.3 %collective-permute-start.5 = (bf16[160,1024]{1,0:T(8,128)(2,1)S(1)}, bf16[160,1024]{1,0:T(8,128)(2,1)}, u32[]{:S(2)}, u32[]{:S(2)}) collective-permute-start(bf16[160,1024]{1,0:T(8,128)(2,1)S(1)} %pad_maximum_fusion.5.refs_6_), channel_id=1, source_target_pairs={{0,128},{16,144},{32,160},{48,176},{64,192},{80,208},{96,224},{112... | collective-permute-start | bytes 983048 | tf_op jit(solution)/shard_map/ppermute | solution.py:298
  9.2 33.7 %collective-permute-start.6 = (bf16[160,1024]{1,0:T(8,128)(2,1)S(1)}, bf16[160,1024]{1,0:T(8,128)(2,1)}, u32[]{:S(2)}, u32[]{:S(2)}) collective-permute-start(bf16[160,1024]{1,0:T(8,128)(2,1)S(1)} %pad_maximum_fusion.5.refs_6_), channel_id=1, source_target_pairs={{0,192},{16,208},{32,224},{48,240},{64,0},{80,16},{96,32},{112,48}... | collective-permute-start | bytes 983048 | tf_op jit(solution)/shard_map/ppermute | solution.py:298
  10.4 14.6 %collective-permute-start = (bf16[96,512]{1,0:T(8,128)(2,1)S(1)}, bf16[96,512]{1,0:T(8,128)(2,1)S(1)}, u32[]{:S(2)}, u32[]{:S(2)}) collective-permute-start(bf16[96,512]{1,0:T(8,128)(2,1)S(1)} %get-tuple-element.26), channel_id=1, source_target_pairs={{0,192},{16,208},{32,224},{48,240},{64,128},{80,144},{96,160},{112... | collective-permute-start | bytes 294920 | tf_op jit(solution)/shard_map/ppermute | solution.py:305
  10.7 22.6 %copy-start.10 = (bf16[1,2048,128]{2,1,0:T(8,128)(2,1)S(1)}, bf16[1,2048,128]{2,1,0:T(8,128)(2,1)}, u32[]{:S(2)}) copy-start(bf16[1,2048,128]{2,1,0:T(8,128)(2,1)} %param.31) | copy-start | bytes 1572868
  25.0 8.3 %copy-start.16 = (bf16[96,1024]{1,0:T(8,128)(2,1)}, bf16[96,1024]{1,0:T(8,128)(2,1)S(1)}, u32[]{:S(2)}) copy-start(bf16[96,1024]{1,0:T(8,128)(2,1)S(1)} %pad_maximum_fusion.7.refs_2_) | copy-start | bytes 589828
  25.0 6.9 %collective-permute-start.1 = (bf16[96,1024]{1,0:T(8,128)(2,1)S(1)}, bf16[96,1024]{1,0:T(8,128)(2,1)S(1)}, u32[]{:S(2)}, u32[]{:S(2)}) collective-permute-start(bf16[96,1024]{1,0:T(8,128)(2,1)S(1)} %pad_maximum_fusion.7.refs_2_), channel_id=1, source_target_pairs={{0,16},{16,32},{32,48},{48,0},{64,80},{80,96},{96,112},{112,64},{1... | collective-permute-start | bytes 589832 | tf_op jit(solution)/shard_map/ppermute | solution.py:291
  26.3 7.1 %copy-start.19 = (s32[64,2]{0,1:T(2,128)S(1)}, s32[64,2]{0,1:T(2,128)}, u32[]{:S(2)}) copy-start(s32[64,2]{0,1:T(2,128)} %param.29) | copy-start | bytes 1540
  26.4 39.8 %copy-start.1 = (bf16[3072,128]{1,0:T(8,128)(2,1)}, bf16[3072,128]{1,0:T(8,128)(2,1)S(1)}, u32[]{:S(2)}) copy-start(bf16[3072,128]{1,0:T(8,128)(2,1)S(1)} %pad_maximum_fusion.1.refs_9_) | copy-start | bytes 2359300
  26.4 10.9 %collective-permute-start.2 = (bf16[96,1024]{1,0:T(8,128)(2,1)S(1)}, bf16[96,1024]{1,0:T(8,128)(2,1)}, u32[]{:S(2)}, u32[]{:S(2)}) collective-permute-start(bf16[96,1024]{1,0:T(8,128)(2,1)S(1)} %pad_maximum_fusion.7.refs_2_), channel_id=1, source_target_pairs={{0,32},{16,48},{32,0},{48,16},{64,96},{80,112},{96,64},{112,80},{1... | collective-permute-start | bytes 589832 | tf_op jit(solution)/shard_map/ppermute | solution.py:291
  32.0 11.0 %copy-start.24 = (bf16[96,1024]{1,0:T(8,128)(2,1)}, bf16[96,1024]{1,0:T(8,128)(2,1)S(1)}, u32[]{:S(2)}) copy-start(bf16[96,1024]{1,0:T(8,128)(2,1)S(1)} %collective-permute-done.1.refs_3_) | copy-start | bytes 589828
  32.0 10.9 %collective-permute-start.3 = (bf16[96,1024]{1,0:T(8,128)(2,1)S(1)}, bf16[96,1024]{1,0:T(8,128)(2,1)}, u32[]{:S(2)}, u32[]{:S(2)}) collective-permute-start(bf16[96,1024]{1,0:T(8,128)(2,1)S(1)} %pad_maximum_fusion.7.refs_2_), channel_id=1, source_target_pairs={{0,48},{16,0},{32,16},{48,32},{64,112},{80,64},{96,80},{112,96},{1... | collective-permute-start | bytes 589832 | tf_op jit(solution)/shard_map/ppermute | solution.py:291
  33.3 44.6 %copy-start.2 = (bf16[3072,128]{1,0:T(8,128)(2,1)}, bf16[3072,128]{1,0:T(8,128)(2,1)S(1)}, u32[]{:S(2)}) copy-start(bf16[3072,128]{1,0:T(8,128)(2,1)S(1)} %pad_maximum_fusion.refs_2_) | copy-start | bytes 2359300
  37.3 60.4 %collective-permute-start.19 = (bf16[3072,128]{1,0:T(8,128)(2,1)S(1)}, bf16[3072,128]{1,0:T(8,128)(2,1)S(1)}, u32[]{:S(2)}, u32[]{:S(2)}) collective-permute-start(bf16[3072,128]{1,0:T(8,128)(2,1)S(1)} %pad_maximum_fusion.1.refs_9_), channel_id=1, source_target_pairs={{0,14},{1,15},{2,0},{3,1},{4,2},{5,3},{6,4},{7,5},{8,6},{9,7},{10,... | collective-permute-start | bytes 2359304 | tf_op jit(solution)/shard_map/ppermute | solution.py:314
  42.8 74.8 %collective-permute-start.18 = (bf16[3072,128]{1,0:T(8,128)(2,1)S(1)}, bf16[3072,128]{1,0:T(8,128)(2,1)}, u32[]{:S(2)}, u32[]{:S(2)}) collective-permute-start(bf16[3072,128]{1,0:T(8,128)(2,1)S(1)} %pad_maximum_fusion.1.refs_9_), channel_id=1, source_target_pairs={{0,2},{1,3},{2,4},{3,5},{4,6},{5,7},{6,8},{7,9},{8,10},{9,11},{10,... | collective-permute-start | bytes 2359304 | tf_op jit(solution)/shard_map/ppermute | solution.py:314
  42.8 0.7 copy-start.23
  42.9 57.4 %collective-permute-start.12 = (bf16[3072,128]{1,0:T(8,128)(2,1)S(1)}, bf16[3072,128]{1,0:T(8,128)(2,1)}, u32[]{:S(2)}, u32[]{:S(2)}) collective-permute-start(bf16[3072,128]{1,0:T(8,128)(2,1)S(1)} %pad_maximum_fusion.refs_2_), channel_id=1, source_target_pairs={{0,2},{1,3},{2,4},{3,5},{4,6},{5,7},{6,8},{7,9},{8,10},{9,11},{10,... | collective-permute-start | bytes 2359304 | tf_op jit(solution)/shard_map/ppermute | solution.py:314
  67.3 10.6 %collective-permute-start.9 = (bf16[80,1024]{1,0:T(8,128)(2,1)S(1)}, bf16[80,1024]{1,0:T(8,128)(2,1)S(1)}, u32[]{:S(2)}, u32[]{:S(2)}) collective-permute-start(bf16[80,1024]{1,0:T(8,128)(2,1)S(1)} %get-tuple-element.15), channel_id=1, source_target_pairs={{0,16},{16,32},{32,48},{48,0},{64,80},{80,96},{96,112},{112,64},{1... | collective-permute-start | bytes 491528 | tf_op jit(solution)/shard_map/ppermute | solution.py:291
  67.8 10.0 %collective-permute-start.8 = (bf16[80,1024]{1,0:T(8,128)(2,1)S(1)}, bf16[80,1024]{1,0:T(8,128)(2,1)S(1)}, u32[]{:S(2)}, u32[]{:S(2)}) collective-permute-start(bf16[80,1024]{1,0:T(8,128)(2,1)S(1)} %get-tuple-element.16), channel_id=1, source_target_pairs={{0,32},{16,48},{32,0},{48,16},{64,96},{80,112},{96,64},{112,80},{1... | collective-permute-start | bytes 491528 | tf_op jit(solution)/shard_map/ppermute | solution.py:291
  77.8 4.8 %collective-permute-start.7 = (bf16[80,1024]{1,0:T(8,128)(2,1)S(1)}, bf16[80,1024]{1,0:T(8,128)(2,1)S(1)}, u32[]{:S(2)}, u32[]{:S(2)}) collective-permute-start(bf16[80,1024]{1,0:T(8,128)(2,1)S(1)} %get-tuple-element.14), channel_id=1, source_target_pairs={{0,48},{16,0},{32,16},{48,32},{64,112},{80,64},{96,80},{112,96},{1... | collective-permute-start | bytes 491528 | tf_op jit(solution)/shard_map/ppermute | solution.py:291
  77.9 39.9 %collective-permute-start.13 = (bf16[3072,128]{1,0:T(8,128)(2,1)S(1)}, bf16[3072,128]{1,0:T(8,128)(2,1)}, u32[]{:S(2)}, u32[]{:S(2)}) collective-permute-start(bf16[3072,128]{1,0:T(8,128)(2,1)S(1)} %pad_maximum_fusion.refs_2_), channel_id=1, source_target_pairs={{0,14},{1,15},{2,0},{3,1},{4,2},{5,3},{6,4},{7,5},{8,6},{9,7},{10,... | collective-permute-start | bytes 2359304 | tf_op jit(solution)/shard_map/ppermute | solution.py:314
  83.7 5.5 %collective-permute-start.10 = (bf16[64,512]{1,0:T(8,128)(2,1)S(1)}, bf16[64,512]{1,0:T(8,128)(2,1)S(1)}, u32[]{:S(2)}, u32[]{:S(2)}) collective-permute-start(bf16[64,512]{1,0:T(8,128)(2,1)S(1)} %get-tuple-element.28), channel_id=1, source_target_pairs={{0,192},{16,208},{32,224},{48,240},{64,128},{80,144},{96,160},{112... | collective-permute-start | bytes 196616 | tf_op jit(solution)/shard_map/ppermute | solution.py:305
  90.4 16.5 %all-to-all-start = ((bf16[16,2,2048]{2,1,0:T(2,128)(2,1)}), bf16[16,2,2048]{2,1,0:T(2,128)(2,1)S(1)}, u32[]{:S(2)}, u32[]{:S(2)}) async-start(bf16[16,2,2048]{2,1,0:T(2,128)(2,1)} %reshape.212), calls=%async_computation | async-start | bytes 262144 | tf_op jit(solution)/shard_map/all_to_all | solution.py:417
  97.6 10.2 %copy-start.14 = (bf16[64,2048]{1,0:T(8,128)(2,1)S(1)}, bf16[64,2048]{1,0:T(8,128)(2,1)}, u32[]{:S(2)}) copy-start(bf16[64,2048]{1,0:T(8,128)(2,1)} %param.27) | copy-start | bytes 786436
  97.6 10.2 %copy-start.18 = (f32[1024]{0:T(1024)S(1)}, f32[1024]{0:T(1024)}, u32[]{:S(2)}) copy-start(f32[1024]{0:T(1024)} %param.25) | copy-start | bytes 12292
  97.6 10.2 %copy-start.4 = (bf16[3072,128]{1,0:T(8,128)(2,1)}, bf16[3072,128]{1,0:T(8,128)(2,1)S(1)}, u32[]{:S(2)}) copy-start(bf16[3072,128]{1,0:T(8,128)(2,1)S(1)} %collective-permute-done.19.refs_11_) | copy-start | bytes 2359300
  97.6 33.2 %collective-permute-start.21 = (bf16[3072,128]{1,0:T(8,128)(2,1)S(1)}, bf16[3072,128]{1,0:T(8,128)(2,1)}, u32[]{:S(2)}, u32[]{:S(2)}) collective-permute-start(bf16[3072,128]{1,0:T(8,128)(2,1)S(1)} %collective-permute-done.19.refs_11_), channel_id=1, source_target_pairs={{0,14},{1,15},{2,0},{3,1},{4,2},{5,3},{6,4},{7,5},{8,6},{9,7},{10,... | collective-permute-start | bytes 2359304 | tf_op jit(solution)/shard_map/ppermute | solution.py:314
  100.3 30.6 %collective-permute-start.14 = (bf16[3072,128]{1,0:T(8,128)(2,1)}, bf16[3072,128]{1,0:T(8,128)(2,1)}, u32[]{:S(2)}, u32[]{:S(2)}) collective-permute-start(bf16[3072,128]{1,0:T(8,128)(2,1)} %collective-permute-done.12.refs_3_), channel_id=1, source_target_pairs={{0,2},{1,3},{2,4},{3,5},{4,6},{5,7},{6,8},{7,9},{8,10},{9,11},{10,... | collective-permute-start | bytes 2359304 | tf_op jit(solution)/shard_map/ppermute | solution.py:314
  107.8 3.2 %copy-start.17 = (f32[2048]{0:T(1024)S(1)}, f32[2048]{0:T(1024)}, u32[]{:S(2)}) copy-start(f32[2048]{0:T(1024)} %param.28) | copy-start | bytes 24580
  112.4 18.4 %all-to-all-start.1 = ((bf16[16,144,128]{2,1,0:T(8,128)(2,1)}), bf16[16,144,128]{2,1,0:T(8,128)(2,1)S(1)}, u32[]{:S(2)}, u32[]{:S(2)}) async-start(bf16[16,144,128]{2,1,0:T(8,128)(2,1)} %pad_maximum_fusion.2), calls=%async_computation.1 | async-start | bytes 1179648 | tf_op jit(solution)/shard_map/all_to_all | solution.py:309
  117.7 21.0 %collective-permute-start.20 = (bf16[3072,128]{1,0:T(8,128)(2,1)}, bf16[3072,128]{1,0:T(8,128)(2,1)}, u32[]{:S(2)}, u32[]{:S(2)}) collective-permute-start(bf16[3072,128]{1,0:T(8,128)(2,1)} %collective-permute-done.18.refs_10_), channel_id=1, source_target_pairs={{0,2},{1,3},{2,4},{3,5},{4,6},{5,7},{6,8},{7,9},{8,10},{9,11},{10,... | collective-permute-start | bytes 2359304 | tf_op jit(solution)/shard_map/ppermute | solution.py:314
  117.8 20.9 %collective-permute-start.15 = (bf16[3072,128]{1,0:T(8,128)(2,1)}, bf16[3072,128]{1,0:T(8,128)(2,1)S(1)}, u32[]{:S(2)}, u32[]{:S(2)}) collective-permute-start(bf16[3072,128]{1,0:T(8,128)(2,1)} %collective-permute-done.13.refs_4_), channel_id=1, source_target_pairs={{0,14},{1,15},{2,0},{3,1},{4,2},{5,3},{6,4},{7,5},{8,6},{9,7},{10,... | collective-permute-start | bytes 2359304 | tf_op jit(solution)/shard_map/ppermute | solution.py:314
  130.8 23.7 %collective-permute-start.23 = (bf16[3072,128]{1,0:T(8,128)(2,1)}, bf16[3072,128]{1,0:T(8,128)(2,1)S(1)}, u32[]{:S(2)}, u32[]{:S(2)}) collective-permute-start(bf16[3072,128]{1,0:T(8,128)(2,1)} %collective-permute-done.21.refs_13_), channel_id=1, source_target_pairs={{0,14},{1,15},{2,0},{3,1},{4,2},{5,3},{6,4},{7,5},{8,6},{9,7},{10,... | collective-permute-start | bytes 2359304 | tf_op jit(solution)/shard_map/ppermute | solution.py:314
  130.9 27.0 %collective-permute-start.16 = (bf16[3072,128]{1,0:T(8,128)(2,1)}, bf16[3072,128]{1,0:T(8,128)(2,1)S(1)}, u32[]{:S(2)}, u32[]{:S(2)}) collective-permute-start(bf16[3072,128]{1,0:T(8,128)(2,1)} %collective-permute-done.14.refs_5_), channel_id=1, source_target_pairs={{0,2},{1,3},{2,4},{3,5},{4,6},{5,7},{6,8},{7,9},{8,10},{9,11},{10,... | collective-permute-start | bytes 2359304 | tf_op jit(solution)/shard_map/ppermute | solution.py:314
  138.7 33.6 %collective-permute-start.22 = (bf16[3072,128]{1,0:T(8,128)(2,1)}, bf16[3072,128]{1,0:T(8,128)(2,1)S(1)}, u32[]{:S(2)}, u32[]{:S(2)}) collective-permute-start(bf16[3072,128]{1,0:T(8,128)(2,1)} %collective-permute-done.20.refs_12_), channel_id=1, source_target_pairs={{0,2},{1,3},{2,4},{3,5},{4,6},{5,7},{6,8},{7,9},{8,10},{9,11},{10,... | collective-permute-start | bytes 2359304 | tf_op jit(solution)/shard_map/ppermute | solution.py:314
  138.7 33.6 %copy-start.5 = (bf16[3072,128]{1,0:T(8,128)(2,1)}, bf16[3072,128]{1,0:T(8,128)(2,1)S(1)}, u32[]{:S(2)}) copy-start(bf16[3072,128]{1,0:T(8,128)(2,1)S(1)} %collective-permute-done.15.refs_6_) | copy-start | bytes 2359300
  138.7 33.6 %collective-permute-start.17 = (bf16[3072,128]{1,0:T(8,128)(2,1)S(1)}, bf16[3072,128]{1,0:T(8,128)(2,1)}, u32[]{:S(2)}, u32[]{:S(2)}) collective-permute-start(bf16[3072,128]{1,0:T(8,128)(2,1)S(1)} %collective-permute-done.15.refs_6_), channel_id=1, source_target_pairs={{0,14},{1,15},{2,0},{3,1},{4,2},{5,3},{6,4},{7,5},{8,6},{9,7},{10,... | collective-permute-start | bytes 2359304 | tf_op jit(solution)/shard_map/ppermute | solution.py:314
  141.4 30.9 %copy-start = (bf16[144,2048]{1,0:T(8,128)(2,1)}, bf16[144,2048]{1,0:T(8,128)(2,1)S(1)}, u32[]{:S(2)}) copy-start(bf16[144,2048]{1,0:T(8,128)(2,1)S(1)} %pad_maximum_fusion.3.refs_0_) | copy-start | bytes 1769476
  141.4 16.4 %collective-permute-start.11 = (bf16[144,2048]{1,0:T(8,128)(2,1)S(1)}, bf16[144,2048]{1,0:T(8,128)(2,1)S(1)}, u32[]{:S(2)}, u32[]{:S(2)}) collective-permute-start(bf16[144,2048]{1,0:T(8,128)(2,1)S(1)} %pad_maximum_fusion.3.refs_0_), channel_id=1, source_target_pairs={{0,1},{1,0},{2,3},{3,2},{4,5},{5,4},{6,7},{7,6},{8,9},{9,8},{10,11... | collective-permute-start | bytes 1769480 | tf_op jit(solution)/shard_map/ppermute | solution.py:319
  154.5 17.8 %copy-start.6 = (bf16[3072,128]{1,0:T(8,128)(2,1)}, bf16[3072,128]{1,0:T(8,128)(2,1)S(1)}, u32[]{:S(2)}) copy-start(bf16[3072,128]{1,0:T(8,128)(2,1)S(1)} %collective-permute-done.23.refs_15_) | copy-start | bytes 2359300
  154.5 33.6 %collective-permute-start.25 = (bf16[3072,128]{1,0:T(8,128)(2,1)S(1)}, bf16[3072,128]{1,0:T(8,128)(2,1)}, u32[]{:S(2)}, u32[]{:S(2)}) collective-permute-start(bf16[3072,128]{1,0:T(8,128)(2,1)S(1)} %collective-permute-done.23.refs_15_), channel_id=1, source_target_pairs={{0,14},{1,15},{2,0},{3,1},{4,2},{5,3},{6,4},{7,5},{8,6},{9,7},{10,... | collective-permute-start | bytes 2359304 | tf_op jit(solution)/shard_map/ppermute | solution.py:314
  157.9 14.5 %copy-start.7 = (bf16[3072,128]{1,0:T(8,128)(2,1)}, bf16[3072,128]{1,0:T(8,128)(2,1)S(1)}, u32[]{:S(2)}) copy-start(bf16[3072,128]{1,0:T(8,128)(2,1)S(1)} %collective-permute-done.16.refs_7_) | copy-start | bytes 2359300
  157.9 31.4 %collective-permute-start.24 = (bf16[3072,128]{1,0:T(8,128)(2,1)S(1)}, bf16[3072,128]{1,0:T(8,128)(2,1)}, u32[]{:S(2)}, u32[]{:S(2)}) collective-permute-start(bf16[3072,128]{1,0:T(8,128)(2,1)S(1)} %collective-permute-done.16.refs_7_), channel_id=1, source_target_pairs={{0,2},{1,3},{2,4},{3,5},{4,6},{5,7},{6,8},{7,9},{8,10},{9,11},{10,... | collective-permute-start | bytes 2359304 | tf_op jit(solution)/shard_map/ppermute | solution.py:314
  157.9 14.5 %copy-start.3 = (bf16[144,2048]{1,0:T(8,128)(2,1)}, bf16[144,2048]{1,0:T(8,128)(2,1)S(1)}, u32[]{:S(2)}) copy-start(bf16[144,2048]{1,0:T(8,128)(2,1)S(1)} %collective-permute-done.11.refs_1_) | copy-start | bytes 1769476
  172.3 0.9 copy-start.8
  195.1 2.5 %collective-permute-start.26 = (bf16[144,2048]{1,0:T(8,128)(2,1)}, bf16[144,2048]{1,0:T(8,128)(2,1)S(1)}, u32[]{:S(2)}, u32[]{:S(2)}) collective-permute-start(bf16[144,2048]{1,0:T(8,128)(2,1)} %get-tuple-element.8), channel_id=1, source_target_pairs={{0,1},{1,0},{2,3},{3,2},{4,5},{5,4},{6,7},{7,6},{8,9},{9,8},{10,11... | collective-permute-start | bytes 1769480 | tf_op jit(solution)/shard_map/ppermute | solution.py:319
  198.8 7.6 %copy-start.20 = (f32[64,2]{0,1:T(2,128)S(1)}, f32[64,2]{0,1:T(2,128)}, u32[]{:S(2)}) copy-start(f32[64,2]{0,1:T(2,128)} %param.30) | copy-start | bytes 1540
  199.7 18.1 %all-to-all-start.2 = ((bf16[16,144,128]{2,1,0:T(8,128)(2,1)}), bf16[16,144,128]{2,1,0:T(8,128)(2,1)S(1)}, u32[]{:S(2)}, u32[]{:S(2)}) async-start(bf16[16,144,128]{2,1,0:T(8,128)(2,1)} %pad_maximum_fusion.4), calls=%async_computation.2 | async-start | bytes 1179648 | tf_op jit(solution)/shard_map/all_to_all | solution.py:309
where the time goes:
time: 220 us; the launch traced here: 219 us
  waiting for transfers between devices  99 us (45%)
  starting transfers between devices  57.5 us (26%)
  Pallas kernels  40.1 us (18%)
  other arithmetic  8.68 us (4%)
  matrix products  6.66 us (3%)
  local copies, waits for them, and re-layouts  6.1 us (3%)
    ppermute x14, waiting for transfers between devices, z_shift(): lax.ppermute(value, 'tp', [(t, (t + CORES * k) % count) for t in range(co...  36.7 us
    pallas_call x1, Pallas kernels, attend(): pl.pallas_call(kernel, out_shape=jax.ShapeDtypeStruct((parts, VH + 16, sp...  22.6 us
    all_to_all x2, waiting for transfers between devices, expert_exchange(): return lax.all_to_all(wire, 'sp', split_axis=0, concat_axis=0, tiled=True)  21.6 us
    ppermute x14, starting transfers between devices, z_shift(): lax.ppermute(value, 'tp', [(t, (t + CORES * k) % count) for t in range(co...  21 us
    pallas_call x2, Pallas kernels, expert_ffn(): pl.pallas_call(kernel, out_shape=outs, in_specs=[vmem, vmem] + [vmem] * l...  17.5 us
    ppermute x6, waiting for transfers between devices, row_shift(): return lax.ppermute(value, 'sp', pairs)  16.8 us
    ppermute x2, waiting for transfers between devices, row_swap(): return lax.ppermute(value, 'sp', pairs)  15.4 us
    all_to_all x2, starting transfers between devices, expert_exchange(): return lax.all_to_all(wire, 'sp', split_axis=0, concat_axis=0, tiled=True)  11.9 us
  transfers between devices with their start and end apart: 30, of which 15 were waited for; matrix products, arithmetic and copies ran while one was open for 6% of the time, Pallas kernels for 16%

commit v1 on v0

--- a/solution.py
+++ b/solution.py
@@ -184,12 +184,9 @@
     return jnp.dot(hidden, down, preferred_element_type=jnp.float32)
 
 
-def expert_kernel(*refs, places, pairs, adds, ends):
+def expert_kernel(x_ref, y_ref, *refs, places, pairs):
     total = len(places)
-    x_ref, y_ref = refs[:2]
-    before, refs = refs[2 : 2 + adds], refs[2 + adds :]
-    w_refs, refs = refs[:total], refs[total:]
-    outs, (acc, w_buf, sems) = refs[:-3], refs[-3:]
+    w_refs, (o_ref, p_ref, acc, w_buf, sems) = refs[:total], refs[total:]
     copies = [
         pltpu.make_async_copy(w_refs[i], w_buf.at[s, pl.ds(first, size)], sems.at[i])
         for i, (s, first, size) in enumerate(places)
@@ -198,57 +195,45 @@
         copy.start()
     rows = jnp.concatenate([x_ref[...], y_ref[...]], axis=0)
     slices = w_buf.shape[0]
-    first = 0
-    while first < slices:
-        slots = list(range(first, min(slices, first + (pairs if slices % pairs == 0 or first else 1))))
+    for first in range(0, slices, pairs):
+        slots = list(range(first, first + pairs))
         for copy, place in zip(copies, places):
             if place[0] in slots:
                 copy.wait()
         part = expert_group(rows, w_buf, slots)
-        if first:
-            part = acc[...] + part
-        elif adds:
-            part = before[0][...] + part
-        acc[...] = part
-        first = slots[-1] + 1
-    if ends:
-        count = x_ref.shape[0]
-        outs[0][...] = acc[:count, :].astype(jnp.bfloat16)
-        outs[1][...] = acc[count:, :].astype(jnp.bfloat16)
-    else:
-        outs[0][...] = acc[...]
-
-
-def expert_ffn(rows, others, before, pieces, places, ends):
+        acc[...] = part if first == 0 else acc[...] + part
+    count = x_ref.shape[0]
+    o_ref[...] = acc[:count, :].astype(jnp.bfloat16)
+    p_ref[...] = acc[count:, :].astype(jnp.bfloat16)
+
+
+def expert_ffn(rows, others, pieces, places):
     count = rows.shape[0]
     slices, depth, width = 1 + max(p[0] for p in places), 3 * D, LANES
     vmem = pl.BlockSpec(memory_space=pltpu.VMEM)
-    hbm = pl.BlockSpec(memory_space=pltpu.HBM)
-    if ends:
-        outs = [jax.ShapeDtypeStruct((count, D), jnp.bfloat16)] * 2
-    else:
-        outs = [jax.ShapeDtypeStruct((2 * count, D), jnp.float32)]
+    hbm = pl.BlockSpec(memory_space=pl.ANY)
 
     def kernel(*refs):
-        expert_kernel(*refs, places=places, pairs=2, adds=len(before), ends=ends)
+        expert_kernel(*refs, places=places, pairs=2)
 
     return pl.pallas_call(
         kernel,
-        out_shape=outs,
-        in_specs=[vmem, vmem] + [vmem] * len(before) + [hbm] * len(pieces),
-        out_specs=[vmem] * len(outs),
+        out_shape=[jax.ShapeDtypeStruct((count, D), jnp.bfloat16)] * 2,
+        in_specs=[vmem, vmem] + [hbm] * len(pieces),
+        out_specs=[vmem, vmem],
         scratch_shapes=[
             pltpu.VMEM((2 * count, D), jnp.float32),
             pltpu.VMEM((slices, depth, width), jnp.bfloat16),
             pltpu.SemaphoreType.DMA((len(pieces),)),
         ],
-        compiler_params=pltpu.CompilerParams(vmem_limit_bytes=58 * 1024 * 1024),
+        compiler_params=pltpu.CompilerParams(vmem_limit_bytes=34 * 1024 * 1024),
         cost_estimate=pl.CostEstimate(
             flops=12 * count * D * slices * width,
             bytes_accessed=6 * D * slices * width,
             transcendentals=2 * count * slices * width,
         ),
-    )(rows, others, *before, *pieces)
+        name="expert_ffn",
+    )(rows, others, *pieces)
 
 
 def to_wire(rows, peers):
@@ -439,11 +424,10 @@
                     continue
                 weight_pieces.append(ring[n])
                 places.append((2 * n - 1 + way if n else 0, start, size))
-    first_sum = expert_ffn(my_rows, their_rows, [], weight_pieces, places, False)
-    last_pieces = [ahead[0][4], behind[1][4]]
     size = halves[0].shape[0]
-    last_places = [(0, 0, size), (0, size, size)]
-    own_sum, other_sum = expert_ffn(my_rows, their_rows, first_sum, last_pieces, last_places, True)
+    weight_pieces += [ahead[0][4], behind[1][4]]
+    places += [(7, 0, size), (7, size, size)]
+    own_sum, other_sum = expert_ffn(my_rows, their_rows, weight_pieces, places)
     served = (
         own_sum.astype(jnp.float32) + core_swap(other_sum).astype(jnp.float32)
     ).astype(jnp.bfloat16)

time: 220 us -> 222 us (level)
  Pallas kernels: 40.1 us -> 28.5 us
  waiting for transfers between devices: 99 us -> 107 us
  local copies, waits for them, and re-layouts: 6.1 us -> 9.89 us
    pallas_call x2 -> x1, Pallas kernels: 17.5 us -> 6.01 us  [expert_ffn(): pl.pallas_call(kernel, out_shape=[jax.ShapeDtypeStruct((count, D), jnp.bf...]
    ppermute x14, waiting for transfers between devices: 36.7 us -> 46.8 us  [z_shift(): lax.ppermute(value, 'tp', [(t, (t + CORES * k) % count) for t in range(co...]
  transfers between devices with their start and end apart: 30 -> 30, of which waited for: 15 -> 16; matrix products, arithmetic and copies ran while one was open for 6% -> 8% of each run, Pallas kernels for 16% -> 10%
where the time goes in v1:
time: 222 us; the launch traced here: 221 us
  waiting for transfers between devices  107 us (48%)
  starting transfers between devices  58.7 us (26%)
  Pallas kernels  28.5 us (13%)
  local copies, waits for them, and re-layouts  9.89 us (4%)
  other arithmetic  8.94 us (4%)
  matrix products  6.69 us (3%)
    ppermute x14, waiting for transfers between devices, z_shift(): lax.ppermute(value, 'tp', [(t, (t + CORES * k) % count) for t in range(co...  46.8 us
    pallas_call x1, Pallas kernels, attend(): pl.pallas_call(kernel, out_shape=jax.ShapeDtypeStruct((parts, VH + 16, sp...  22.5 us
    ppermute x14, starting transfers between devices, z_shift(): lax.ppermute(value, 'tp', [(t, (t + CORES * k) % count) for t in range(co...  21 us
    all_to_all x2, waiting for transfers between devices, expert_exchange(): return lax.all_to_all(wire, 'sp', split_axis=0, concat_axis=0, tiled=True)  19.9 us
    ppermute x6, waiting for transfers between devices, row_shift(): return lax.ppermute(value, 'sp', pairs)  15.9 us
    ppermute x2, waiting for transfers between devices, row_swap(): return lax.ppermute(value, 'sp', pairs)  15.5 us
    all_to_all x2, starting transfers between devices, expert_exchange(): return lax.all_to_all(wire, 'sp', split_axis=0, concat_axis=0, tiled=True)  12 us
    all_to_all x1, starting transfers between devices, shards(): lax.all_to_all(attended.T, 'tp', split_axis=0, concat_axis=1, tiled=True)  8.01 us
  transfers between devices with their start and end apart: 30, of which 16 were waited for; matrix products, arithmetic and copies ran while one was open for 8% of the time, Pallas kernels for 10%

profile of v1, /device:TPU:1, one launch (start us, length us, event | category | flops | bytes accessed | tf_op | source)
XLA Modules:
  0.0 220.9 jit_solution(4462206628005833544)
XLA Ops:
  0.0 1.5 fusion.1
  1.6 2.0 convolution_convert_fusion.1
  4.0 0.3 fusion.42
  4.4 2.2 collective-permute-start.4
  6.6 2.6 %collective-permute-start.5 = (bf16[160,1024]{1,0:T(8,128)(2,1)S(1)}, bf16[160,1024]{1,0:T(8,128)(2,1)}, u32[]{:S(2)}, u32[]{:S(2)}) collective-permute-start(bf16[160,1024]{1,0:T(8,128)(2,1)S(1)} %pad_maximum_fusion.5.refs_6_), channel_id=1, source_target_pairs={{0,128},{16,144},{32,160},{48,176},{64,192},{80,208},{96,224},{112... | collective-permute-start | bytes 983048 | tf_op jit(solution)/shard_map/ppermute | solution.py:283
  9.2 1.1 collective-permute-start.6
  10.8 14.2 %collective-permute-done = bf16[96,512]{1,0:T(8,128)(2,1)S(1)} collective-permute-done((bf16[96,512]{1,0:T(8,128)(2,1)S(1)}, bf16[96,512]{1,0:T(8,128)(2,1)S(1)}, u32[]{:S(2)}, u32[]{:S(2)}) %collective-permute-start) | collective-permute-done | bytes 98336 | tf_op jit(solution)/shard_map/ppermute | solution.py:290
  25.0 1.3 collective-permute-start.1
  26.4 2.5 %collective-permute-start.2 = (bf16[96,1024]{1,0:T(8,128)(2,1)S(1)}, bf16[96,1024]{1,0:T(8,128)(2,1)S(1)}, u32[]{:S(2)}, u32[]{:S(2)}) collective-permute-start(bf16[96,1024]{1,0:T(8,128)(2,1)S(1)} %pad_maximum_fusion.7.refs_2_), channel_id=1, source_target_pairs={{0,32},{16,48},{32,0},{48,16},{64,96},{80,112},{96,64},{112,80},{1... | collective-permute-start | bytes 589832 | tf_op jit(solution)/shard_map/ppermute | solution.py:276
  28.9 3.0 %collective-permute-done.1.refs_3_ = bf16[96,1024]{1,0:T(8,128)(2,1)S(1)} collective-permute-done((bf16[96,1024]{1,0:T(8,128)(2,1)S(1)}, bf16[96,1024]{1,0:T(8,128)(2,1)S(1)}, u32[]{:S(2)}, u32[]{:S(2)}) %collective-permute-start.1) | collective-permute-done | bytes 196640 | tf_op jit(solution)/shard_map/ppermute | solution.py:276
  32.0 1.3 collective-permute-start.3
  33.7 0.7 stack.50.refs_0_
  34.4 0.6 pad_add_fusion.refs_1_
  35.0 2.1 collective-permute-done.2.refs_4_
  37.2 5.6 %collective-permute-start.19 = (bf16[3072,128]{1,0:T(8,128)(2,1)S(1)}, bf16[3072,128]{1,0:T(8,128)(2,1)S(1)}, u32[]{:S(2)}, u32[]{:S(2)}) collective-permute-start(bf16[3072,128]{1,0:T(8,128)(2,1)S(1)} %pad_maximum_fusion.1.refs_9_), channel_id=1, source_target_pairs={{0,14},{1,15},{2,0},{3,1},{4,2},{5,3},{6,4},{7,5},{8,6},{9,7},{10,... | collective-permute-start | bytes 2359304 | tf_op jit(solution)/shard_map/ppermute | solution.py:299
  42.9 22.5 %attend.1 = bf16[4,80,1024]{2,1,0:T(8,128)(2,1)} custom-call(s32[8]{0:T(128)} %stack.50.refs_0_, s32[4]{0:T(128)} %pad_add_fusion.refs_1_, bf16[96,1024]{1,0:T(8,128)(2,1)} %copy-done.8, bf16[96,1024]{1,0:T(8,128)(2,1)} %copy-done.16, bf16[96,1024]{1,0:T(8,128)(2,1)} %copy-done.17, bf16[96,1024]{1,0:T(8,128)(2,1)} %collective-permute-done.3.refs_5_, ...), custom_call_target="tpu_custom_call" | custom-call | flops 2684354560 | bytes 3145728 | tf_op jit(solution)/shard_map/attend/pallas_call | solution.py:144
  65.4 1.8 slice_bitcast_fusion.8
  67.3 0.2 reduce_window_sum.11
  67.6 0.7 convert_reduce_fusion.3
  68.3 9.4 %collective-permute-done.9 = bf16[80,1024]{1,0:T(8,128)(2,1)} collective-permute-done((bf16[80,1024]{1,0:T(8,128)(2,1)}, bf16[80,1024]{1,0:T(8,128)(2,1)}, u32[]{:S(2)}, u32[]{:S(2)}) %collective-permute-start.9) | collective-permute-done | bytes 163872 | tf_op jit(solution)/shard_map/ppermute | solution.py:276
  77.8 0.7 convert_reduce_fusion
  78.5 2.5 %collective-permute-start.13 = (bf16[3072,128]{1,0:T(8,128)(2,1)S(1)}, bf16[3072,128]{1,0:T(8,128)(2,1)}, u32[]{:S(2)}, u32[]{:S(2)}) collective-permute-start(bf16[3072,128]{1,0:T(8,128)(2,1)S(1)} %pad_maximum_fusion.refs_2_), channel_id=1, source_target_pairs={{0,14},{1,15},{2,0},{3,1},{4,2},{5,3},{6,4},{7,5},{8,6},{9,7},{10,... | collective-permute-start | bytes 2359304 | tf_op jit(solution)/shard_map/ppermute | solution.py:299
  81.0 1.4 collective-permute-done.7
  82.4 1.1 fusion.22
  83.5 3.9 %collective-permute-start.10 = (bf16[64,512]{1,0:T(8,128)(2,1)S(1)}, bf16[64,512]{1,0:T(8,128)(2,1)S(1)}, u32[]{:S(2)}, u32[]{:S(2)}) collective-permute-start(bf16[64,512]{1,0:T(8,128)(2,1)S(1)} %get-tuple-element.28), channel_id=1, source_target_pairs={{0,192},{16,208},{32,224},{48,240},{64,128},{80,144},{96,160},{112... | collective-permute-start | bytes 196616 | tf_op jit(solution)/shard_map/ppermute | solution.py:290
  87.4 0.2 select_reduce_fusion.1
  87.8 1.3 collective-permute-done.10
  89.1 0.2 copy.57
  89.3 0.9 reshape.212
  90.2 8.0 %all-to-all-start = ((bf16[16,2,2048]{2,1,0:T(2,128)(2,1)}), bf16[16,2,2048]{2,1,0:T(2,128)(2,1)S(1)}, u32[]{:S(2)}, u32[]{:S(2)}) async-start(bf16[16,2,2048]{2,1,0:T(2,128)(2,1)} %reshape.212), calls=%async_computation | async-start | bytes 262144 | tf_op jit(solution)/shard_map/all_to_all | solution.py:402
  98.2 0.7 fusion.45
  98.9 2.6 %collective-permute-start.21 = (bf16[3072,128]{1,0:T(8,128)(2,1)S(1)}, bf16[3072,128]{1,0:T(8,128)(2,1)}, u32[]{:S(2)}, u32[]{:S(2)}) collective-permute-start(bf16[3072,128]{1,0:T(8,128)(2,1)S(1)} %collective-permute-done.19.refs_11_), channel_id=1, source_target_pairs={{0,14},{1,15},{2,0},{3,1},{4,2},{5,3},{6,4},{7,5},{8,6},{9,7},{10,... | collective-permute-start | bytes 2359304 | tf_op jit(solution)/shard_map/ppermute | solution.py:299
  101.5 6.0 %all-to-all-done = bf16[16,2,2048]{2,1,0:T(2,128)(2,1)S(1)} async-done(((bf16[16,2,2048]{2,1,0:T(2,128)(2,1)}), bf16[16,2,2048]{2,1,0:T(2,128)(2,1)S(1)}, u32[]{:S(2)}, u32[]{:S(2)}) %all-to-all-start) | async-done | bytes 131104 | tf_op jit(solution)/shard_map/all_to_all | solution.py:402
  107.4 0.2 reshape.213
  107.7 0.2 fusion.10
  107.9 1.1 copy.52
  109.0 1.2 reshape.211
  110.2 3.2 %multiply_reduce_fusion = (f32[64]{0:T(128)S(1)}, f32[64,2048]{1,0:T(8,128)S(1)}) fusion(bf16[1024,2048]{1,0:T(8,128)(2,1)} %param.26, f32[64,1024]{1,0:T(8,128)S(1)} %reshape.211, f32[1024]{0:T(1024)S(1)} %copy-done.11, f32[64]{0:T(128)S(1)} %add_rsqrt_fusion.4, bf16[64,2048]{1,0:T(8,128)(2,1)} %param.27), kind=kOutput, calls=%fused_computation.29 | convolution fusion | flops 269156288 | bytes 5247488 | tf_op jit(solution)/shard_map/dot_general | solution.py:405
  113.5 0.8 copy-done
  114.2 0.4 convolution_convert_fusion
  114.7 0.9 pad_maximum_fusion.2
  115.6 5.3 %all-to-all-start.1 = ((bf16[16,144,128]{2,1,0:T(8,128)(2,1)}), bf16[16,144,128]{2,1,0:T(8,128)(2,1)}, u32[]{:S(2)}, u32[]{:S(2)}) async-start(bf16[16,144,128]{2,1,0:T(8,128)(2,1)} %pad_maximum_fusion.2), calls=%async_computation.1 | async-start | bytes 1179648 | tf_op jit(solution)/shard_map/all_to_all | solution.py:294
  121.0 2.7 %collective-permute-start.15 = (bf16[3072,128]{1,0:T(8,128)(2,1)}, bf16[3072,128]{1,0:T(8,128)(2,1)}, u32[]{:S(2)}, u32[]{:S(2)}) collective-permute-start(bf16[3072,128]{1,0:T(8,128)(2,1)} %collective-permute-done.13.refs_4_), channel_id=1, source_target_pairs={{0,14},{1,15},{2,0},{3,1},{4,2},{5,3},{6,4},{7,5},{8,6},{9,7},{10,... | collective-permute-start | bytes 2359304 | tf_op jit(solution)/shard_map/ppermute | solution.py:299
  123.7 1.4 collective-permute-start.16
  125.1 8.6 %all-to-all-done.1 = bf16[16,144,128]{2,1,0:T(8,128)(2,1)} async-done(((bf16[16,144,128]{2,1,0:T(8,128)(2,1)}), bf16[16,144,128]{2,1,0:T(8,128)(2,1)}, u32[]{:S(2)}, u32[]{:S(2)}) %all-to-all-start.1) | async-done | bytes 589856 | tf_op jit(solution)/shard_map/all_to_all | solution.py:294
  133.7 0.8 slice.173
  134.6 1.1 slice_bitcast_fusion.2
  135.7 5.9 %collective-permute-done.20.refs_12_ = bf16[3072,128]{1,0:T(8,128)(2,1)} collective-permute-done((bf16[3072,128]{1,0:T(8,128)(2,1)S(1)}, bf16[3072,128]{1,0:T(8,128)(2,1)}, u32[]{:S(2)}, u32[]{:S(2)}) %collective-permute-start.20) | collective-permute-done | bytes 786464 | tf_op jit(solution)/shard_map/ppermute | solution.py:299
  141.6 2.7 %collective-permute-start.17 = (bf16[3072,128]{1,0:T(8,128)(2,1)}, bf16[3072,128]{1,0:T(8,128)(2,1)S(1)}, u32[]{:S(2)}, u32[]{:S(2)}) collective-permute-start(bf16[3072,128]{1,0:T(8,128)(2,1)} %collective-permute-done.15.refs_6_), channel_id=1, source_target_pairs={{0,14},{1,15},{2,0},{3,1},{4,2},{5,3},{6,4},{7,5},{8,6},{9,7},{10,... | collective-permute-start | bytes 2359304 | tf_op jit(solution)/shard_map/ppermute | solution.py:299
  144.3 13.4 %collective-permute-done.23.refs_15_ = bf16[3072,128]{1,0:T(8,128)(2,1)} collective-permute-done((bf16[3072,128]{1,0:T(8,128)(2,1)}, bf16[3072,128]{1,0:T(8,128)(2,1)}, u32[]{:S(2)}, u32[]{:S(2)}) %collective-permute-start.23) | collective-permute-done | bytes 786464 | tf_op jit(solution)/shard_map/ppermute | solution.py:299
  157.6 3.4 %collective-permute-start.25 = (bf16[3072,128]{1,0:T(8,128)(2,1)}, bf16[3072,128]{1,0:T(8,128)(2,1)S(1)}, u32[]{:S(2)}, u32[]{:S(2)}) collective-permute-start(bf16[3072,128]{1,0:T(8,128)(2,1)} %collective-permute-done.23.refs_15_), channel_id=1, source_target_pairs={{0,14},{1,15},{2,0},{3,1},{4,2},{5,3},{6,4},{7,5},{8,6},{9,7},{10,... | collective-permute-start | bytes 2359304 | tf_op jit(solution)/shard_map/ppermute | solution.py:299
  161.1 1.8 collective-permute-start.11
  162.9 1.6 collective-permute-done.11.refs_1_
  164.6 10.6 %collective-permute-done.22.refs_14_ = bf16[3072,128]{1,0:T(8,128)(2,1)S(1)} collective-permute-done((bf16[3072,128]{1,0:T(8,128)(2,1)}, bf16[3072,128]{1,0:T(8,128)(2,1)S(1)}, u32[]{:S(2)}, u32[]{:S(2)}) %collective-permute-start.22) | collective-permute-done | bytes 786464 | tf_op jit(solution)/shard_map/ppermute | solution.py:299
  175.2 16.2 %collective-permute-done.25.refs_17_ = bf16[3072,128]{1,0:T(8,128)(2,1)S(1)} collective-permute-done((bf16[3072,128]{1,0:T(8,128)(2,1)}, bf16[3072,128]{1,0:T(8,128)(2,1)S(1)}, u32[]{:S(2)}, u32[]{:S(2)}) %collective-permute-start.25) | collective-permute-done | bytes 786464 | tf_op jit(solution)/shard_map/ppermute | solution.py:299
  191.4 0.7 collective-permute-done.24.refs_16_
  192.0 6.0 %expert_ffn.1 = (bf16[144,2048]{1,0:T(8,128)(2,1)S(1)}, bf16[144,2048]{1,0:T(8,128)(2,1)S(1)}) custom-call(bf16[144,2048]{1,0:T(8,128)(2,1)S(1)} %pad_maximum_fusion.3.refs_0_, bf16[144,2048]{1,0:T(8,128)(2,1)S(1)} %collective-permute-done.11.refs_1_, bf16[3072,128]{1,0:T(8,128)(2,1)S(1)} %pad_maximum_fusion.refs_2_, ...), custom_call_target="tpu_custom_call" | custom-call | flops 3623878656 | bytes 12582912 | tf_op jit(solution)/shard_map/expert_ffn/pallas_call | solution.py:219
  198.1 0.7 collective-permute-start.26
  198.8 1.6 collective-permute-done.26
  200.4 0.1 add_convert_fusion
  200.7 0.9 pad_maximum_fusion.4
  201.5 6.7 %all-to-all-start.2 = ((bf16[16,144,128]{2,1,0:T(8,128)(2,1)}), bf16[16,144,128]{2,1,0:T(8,128)(2,1)S(1)}, u32[]{:S(2)}, u32[]{:S(2)}) async-start(bf16[16,144,128]{2,1,0:T(8,128)(2,1)} %pad_maximum_fusion.4), calls=%async_computation.2 | async-start | bytes 1179648 | tf_op jit(solution)/shard_map/all_to_all | solution.py:294
  208.4 11.3 %all-to-all-done.2 = bf16[16,144,128]{2,1,0:T(8,128)(2,1)S(1)} async-done(((bf16[16,144,128]{2,1,0:T(8,128)(2,1)}), bf16[16,144,128]{2,1,0:T(8,128)(2,1)S(1)}, u32[]{:S(2)}, u32[]{:S(2)}) %all-to-all-start.2) | async-done | bytes 589856 | tf_op jit(solution)/shard_map/all_to_all | solution.py:294
  219.8 1.1 fusion
  (107 shorter events, 2.4 us)
Async XLA Ops:
  1.5 2.1 copy-start.7
  1.5 2.2 copy-start.2
  1.5 2.2 %copy-start.14 = (f32[96]{0:T(128)S(1)}, f32[96]{0:T(128)}, u32[]{:S(2)}) copy-start(f32[96]{0:T(128)} %param.24) | copy-start | bytes 1156
  1.6 2.4 %copy-start.15 = (f32[96]{0:T(128)S(1)}, f32[96]{0:T(128)}, u32[]{:S(2)}) copy-start(f32[96]{0:T(128)} %param.23) | copy-start | bytes 1156
  3.9 6.6 %copy-start.4 = (bf16[1,2048,128]{2,1,0:T(8,128)(2,1)S(1)}, bf16[1,2048,128]{2,1,0:T(8,128)(2,1)}, u32[]{:S(2)}) copy-start(bf16[1,2048,128]{2,1,0:T(8,128)(2,1)} %param.32) | copy-start | bytes 1572868
  4.0 6.5 %copy-start.5 = (bf16[1,128,2048]{2,1,0:T(8,128)(2,1)S(1)}, bf16[1,128,2048]{2,1,0:T(8,128)(2,1)}, u32[]{:S(2)}) copy-start(bf16[1,128,2048]{2,1,0:T(8,128)(2,1)} %param.33) | copy-start | bytes 1572868
  4.4 6.2 %copy-start.6 = (bf16[160,1024]{1,0:T(8,128)(2,1)}, bf16[160,1024]{1,0:T(8,128)(2,1)S(1)}, u32[]{:S(2)}) copy-start(bf16[160,1024]{1,0:T(8,128)(2,1)S(1)} %pad_maximum_fusion.5.refs_6_) | copy-start | bytes 983044
  4.4 38.3 %collective-permute-start.4 = (bf16[160,1024]{1,0:T(8,128)(2,1)S(1)}, bf16[160,1024]{1,0:T(8,128)(2,1)}, u32[]{:S(2)}, u32[]{:S(2)}) collective-permute-start(bf16[160,1024]{1,0:T(8,128)(2,1)S(1)} %pad_maximum_fusion.5.refs_6_), channel_id=1, source_target_pairs={{0,64},{16,80},{32,96},{48,112},{64,128},{80,144},{96,160},{112,17... | collective-permute-start | bytes 983048 | tf_op jit(solution)/shard_map/ppermute | solution.py:283
  6.6 36.2 %collective-permute-start.5 = (bf16[160,1024]{1,0:T(8,128)(2,1)S(1)}, bf16[160,1024]{1,0:T(8,128)(2,1)}, u32[]{:S(2)}, u32[]{:S(2)}) collective-permute-start(bf16[160,1024]{1,0:T(8,128)(2,1)S(1)} %pad_maximum_fusion.5.refs_6_), channel_id=1, source_target_pairs={{0,128},{16,144},{32,160},{48,176},{64,192},{80,208},{96,224},{112... | collective-permute-start | bytes 983048 | tf_op jit(solution)/shard_map/ppermute | solution.py:283
  9.2 33.6 %collective-permute-start.6 = (bf16[160,1024]{1,0:T(8,128)(2,1)S(1)}, bf16[160,1024]{1,0:T(8,128)(2,1)}, u32[]{:S(2)}, u32[]{:S(2)}) collective-permute-start(bf16[160,1024]{1,0:T(8,128)(2,1)S(1)} %pad_maximum_fusion.5.refs_6_), channel_id=1, source_target_pairs={{0,192},{16,208},{32,224},{48,240},{64,0},{80,16},{96,32},{112,48}... | collective-permute-start | bytes 983048 | tf_op jit(solution)/shard_map/ppermute | solution.py:283
  10.4 14.6 %collective-permute-start = (bf16[96,512]{1,0:T(8,128)(2,1)S(1)}, bf16[96,512]{1,0:T(8,128)(2,1)S(1)}, u32[]{:S(2)}, u32[]{:S(2)}) collective-permute-start(bf16[96,512]{1,0:T(8,128)(2,1)S(1)} %get-tuple-element.26), channel_id=1, source_target_pairs={{0,192},{16,208},{32,224},{48,240},{64,128},{80,144},{96,160},{112... | collective-permute-start | bytes 294920 | tf_op jit(solution)/shard_map/ppermute | solution.py:290
  10.7 22.6 %copy-start.3 = (bf16[1,2048,128]{2,1,0:T(8,128)(2,1)S(1)}, bf16[1,2048,128]{2,1,0:T(8,128)(2,1)}, u32[]{:S(2)}) copy-start(bf16[1,2048,128]{2,1,0:T(8,128)(2,1)} %param.31) | copy-start | bytes 1572868
  25.0 8.3 %copy-start.8 = (bf16[96,1024]{1,0:T(8,128)(2,1)}, bf16[96,1024]{1,0:T(8,128)(2,1)S(1)}, u32[]{:S(2)}) copy-start(bf16[96,1024]{1,0:T(8,128)(2,1)S(1)} %pad_maximum_fusion.7.refs_2_) | copy-start | bytes 589828
  25.0 6.9 %collective-permute-start.1 = (bf16[96,1024]{1,0:T(8,128)(2,1)S(1)}, bf16[96,1024]{1,0:T(8,128)(2,1)S(1)}, u32[]{:S(2)}, u32[]{:S(2)}) collective-permute-start(bf16[96,1024]{1,0:T(8,128)(2,1)S(1)} %pad_maximum_fusion.7.refs_2_), channel_id=1, source_target_pairs={{0,16},{16,32},{32,48},{48,0},{64,80},{80,96},{96,112},{112,64},{1... | collective-permute-start | bytes 589832 | tf_op jit(solution)/shard_map/ppermute | solution.py:276
  26.3 7.1 %copy-start.12 = (s32[64,2]{0,1:T(2,128)S(1)}, s32[64,2]{0,1:T(2,128)}, u32[]{:S(2)}) copy-start(s32[64,2]{0,1:T(2,128)} %param.29) | copy-start | bytes 1540
  26.4 10.8 %collective-permute-start.2 = (bf16[96,1024]{1,0:T(8,128)(2,1)S(1)}, bf16[96,1024]{1,0:T(8,128)(2,1)S(1)}, u32[]{:S(2)}, u32[]{:S(2)}) collective-permute-start(bf16[96,1024]{1,0:T(8,128)(2,1)S(1)} %pad_maximum_fusion.7.refs_2_), channel_id=1, source_target_pairs={{0,32},{16,48},{32,0},{48,16},{64,96},{80,112},{96,64},{112,80},{1... | collective-permute-start | bytes 589832 | tf_op jit(solution)/shard_map/ppermute | solution.py:276
  32.0 1.5 copy-start.16
  32.0 10.8 %collective-permute-start.3 = (bf16[96,1024]{1,0:T(8,128)(2,1)S(1)}, bf16[96,1024]{1,0:T(8,128)(2,1)}, u32[]{:S(2)}, u32[]{:S(2)}) collective-permute-start(bf16[96,1024]{1,0:T(8,128)(2,1)S(1)} %pad_maximum_fusion.7.refs_2_), channel_id=1, source_target_pairs={{0,48},{16,0},{32,16},{48,32},{64,112},{80,64},{96,80},{112,96},{1... | collective-permute-start | bytes 589832 | tf_op jit(solution)/shard_map/ppermute | solution.py:276
  37.2 5.6 %copy-start.17 = (bf16[96,1024]{1,0:T(8,128)(2,1)}, bf16[96,1024]{1,0:T(8,128)(2,1)S(1)}, u32[]{:S(2)}) copy-start(bf16[96,1024]{1,0:T(8,128)(2,1)S(1)} %collective-permute-done.2.refs_4_) | copy-start | bytes 589828
  37.2 61.7 %collective-permute-start.19 = (bf16[3072,128]{1,0:T(8,128)(2,1)S(1)}, bf16[3072,128]{1,0:T(8,128)(2,1)S(1)}, u32[]{:S(2)}, u32[]{:S(2)}) collective-permute-start(bf16[3072,128]{1,0:T(8,128)(2,1)S(1)} %pad_maximum_fusion.1.refs_9_), channel_id=1, source_target_pairs={{0,14},{1,15},{2,0},{3,1},{4,2},{5,3},{6,4},{7,5},{8,6},{9,7},{10,... | collective-permute-start | bytes 2359304 | tf_op jit(solution)/shard_map/ppermute | solution.py:299
  42.7 78.1 %collective-permute-start.18 = (bf16[3072,128]{1,0:T(8,128)(2,1)S(1)}, bf16[3072,128]{1,0:T(8,128)(2,1)S(1)}, u32[]{:S(2)}, u32[]{:S(2)}) collective-permute-start(bf16[3072,128]{1,0:T(8,128)(2,1)S(1)} %pad_maximum_fusion.1.refs_9_), channel_id=1, source_target_pairs={{0,2},{1,3},{2,4},{3,5},{4,6},{5,7},{6,8},{7,9},{8,10},{9,11},{10,... | collective-permute-start | bytes 2359304 | tf_op jit(solution)/shard_map/ppermute | solution.py:299
  42.8 58.7 %collective-permute-start.12 = (bf16[3072,128]{1,0:T(8,128)(2,1)S(1)}, bf16[3072,128]{1,0:T(8,128)(2,1)}, u32[]{:S(2)}, u32[]{:S(2)}) collective-permute-start(bf16[3072,128]{1,0:T(8,128)(2,1)S(1)} %pad_maximum_fusion.refs_2_), channel_id=1, source_target_pairs={{0,2},{1,3},{2,4},{3,5},{4,6},{5,7},{6,8},{7,9},{8,10},{9,11},{10,... | collective-permute-start | bytes 2359304 | tf_op jit(solution)/shard_map/ppermute | solution.py:299
  67.2 10.5 %collective-permute-start.9 = (bf16[80,1024]{1,0:T(8,128)(2,1)}, bf16[80,1024]{1,0:T(8,128)(2,1)}, u32[]{:S(2)}, u32[]{:S(2)}) collective-permute-start(bf16[80,1024]{1,0:T(8,128)(2,1)} %get-tuple-element.15), channel_id=1, source_target_pairs={{0,16},{16,32},{32,48},{48,0},{64,80},{80,96},{96,112},{112,64},{1... | collective-permute-start | bytes 491528 | tf_op jit(solution)/shard_map/ppermute | solution.py:276
  67.5 11.0 %collective-permute-start.8 = (bf16[80,1024]{1,0:T(8,128)(2,1)}, bf16[80,1024]{1,0:T(8,128)(2,1)S(1)}, u32[]{:S(2)}, u32[]{:S(2)}) collective-permute-start(bf16[80,1024]{1,0:T(8,128)(2,1)} %get-tuple-element.16), channel_id=1, source_target_pairs={{0,32},{16,48},{32,0},{48,16},{64,96},{80,112},{96,64},{112,80},{1... | collective-permute-start | bytes 491528 | tf_op jit(solution)/shard_map/ppermute | solution.py:276
  77.8 4.6 %collective-permute-start.7 = (bf16[80,1024]{1,0:T(8,128)(2,1)S(1)}, bf16[80,1024]{1,0:T(8,128)(2,1)S(1)}, u32[]{:S(2)}, u32[]{:S(2)}) collective-permute-start(bf16[80,1024]{1,0:T(8,128)(2,1)S(1)} %get-tuple-element.14), channel_id=1, source_target_pairs={{0,48},{16,0},{32,16},{48,32},{64,112},{80,64},{96,80},{112,96},{1... | collective-permute-start | bytes 491528 | tf_op jit(solution)/shard_map/ppermute | solution.py:276
  78.5 42.5 %collective-permute-start.13 = (bf16[3072,128]{1,0:T(8,128)(2,1)S(1)}, bf16[3072,128]{1,0:T(8,128)(2,1)}, u32[]{:S(2)}, u32[]{:S(2)}) collective-permute-start(bf16[3072,128]{1,0:T(8,128)(2,1)S(1)} %pad_maximum_fusion.refs_2_), channel_id=1, source_target_pairs={{0,14},{1,15},{2,0},{3,1},{4,2},{5,3},{6,4},{7,5},{8,6},{9,7},{10,... | collective-permute-start | bytes 2359304 | tf_op jit(solution)/shard_map/ppermute | solution.py:299
  83.5 5.5 %collective-permute-start.10 = (bf16[64,512]{1,0:T(8,128)(2,1)S(1)}, bf16[64,512]{1,0:T(8,128)(2,1)S(1)}, u32[]{:S(2)}, u32[]{:S(2)}) collective-permute-start(bf16[64,512]{1,0:T(8,128)(2,1)S(1)} %get-tuple-element.28), channel_id=1, source_target_pairs={{0,192},{16,208},{32,224},{48,240},{64,128},{80,144},{96,160},{112... | collective-permute-start | bytes 196616 | tf_op jit(solution)/shard_map/ppermute | solution.py:290
  90.2 17.3 %all-to-all-start = ((bf16[16,2,2048]{2,1,0:T(2,128)(2,1)}), bf16[16,2,2048]{2,1,0:T(2,128)(2,1)S(1)}, u32[]{:S(2)}, u32[]{:S(2)}) async-start(bf16[16,2,2048]{2,1,0:T(2,128)(2,1)} %reshape.212), calls=%async_computation | async-start | bytes 262144 | tf_op jit(solution)/shard_map/all_to_all | solution.py:402
  98.9 11.3 %copy-start.11 = (f32[1024]{0:T(1024)S(1)}, f32[1024]{0:T(1024)}, u32[]{:S(2)}) copy-start(f32[1024]{0:T(1024)} %param.25) | copy-start | bytes 12292
  98.9 24.8 %collective-permute-start.21 = (bf16[3072,128]{1,0:T(8,128)(2,1)S(1)}, bf16[3072,128]{1,0:T(8,128)(2,1)}, u32[]{:S(2)}, u32[]{:S(2)}) collective-permute-start(bf16[3072,128]{1,0:T(8,128)(2,1)S(1)} %collective-permute-done.19.refs_11_), channel_id=1, source_target_pairs={{0,14},{1,15},{2,0},{3,1},{4,2},{5,3},{6,4},{7,5},{8,6},{9,7},{10,... | collective-permute-start | bytes 2359304 | tf_op jit(solution)/shard_map/ppermute | solution.py:299
  101.5 22.3 %collective-permute-start.14 = (bf16[3072,128]{1,0:T(8,128)(2,1)}, bf16[3072,128]{1,0:T(8,128)(2,1)}, u32[]{:S(2)}, u32[]{:S(2)}) collective-permute-start(bf16[3072,128]{1,0:T(8,128)(2,1)} %collective-permute-done.12.refs_3_), channel_id=1, source_target_pairs={{0,2},{1,3},{2,4},{3,5},{4,6},{5,7},{6,8},{7,9},{8,10},{9,11},{10,... | collective-permute-start | bytes 2359304 | tf_op jit(solution)/shard_map/ppermute | solution.py:299
  110.2 4.1 %copy-start.9 = (bf16[64,144]{1,0:T(8,128)(2,1)S(1)}, bf16[64,144]{1,0:T(8,128)(2,1)}, u32[]{:S(2)}) copy-start(bf16[64,144]{1,0:T(8,128)(2,1)} %fusion.45) | copy-start | bytes 55300
  110.2 4.1 %copy-start.10 = (f32[2048]{0:T(1024)S(1)}, f32[2048]{0:T(1024)}, u32[]{:S(2)}) copy-start(f32[2048]{0:T(1024)} %param.28) | copy-start | bytes 24580
  113.4 0.8 copy-start
  115.6 18.2 %all-to-all-start.1 = ((bf16[16,144,128]{2,1,0:T(8,128)(2,1)}), bf16[16,144,128]{2,1,0:T(8,128)(2,1)}, u32[]{:S(2)}, u32[]{:S(2)}) async-start(bf16[16,144,128]{2,1,0:T(8,128)(2,1)} %pad_maximum_fusion.2), calls=%async_computation.1 | async-start | bytes 1179648 | tf_op jit(solution)/shard_map/all_to_all | solution.py:294
  120.9 20.7 %collective-permute-start.20 = (bf16[3072,128]{1,0:T(8,128)(2,1)S(1)}, bf16[3072,128]{1,0:T(8,128)(2,1)}, u32[]{:S(2)}, u32[]{:S(2)}) collective-permute-start(bf16[3072,128]{1,0:T(8,128)(2,1)S(1)} %collective-permute-done.18.refs_10_), channel_id=1, source_target_pairs={{0,2},{1,3},{2,4},{3,5},{4,6},{5,7},{6,8},{7,9},{8,10},{9,11},{10,... | collective-permute-start | bytes 2359304 | tf_op jit(solution)/shard_map/ppermute | solution.py:299
  121.0 20.6 %collective-permute-start.15 = (bf16[3072,128]{1,0:T(8,128)(2,1)}, bf16[3072,128]{1,0:T(8,128)(2,1)}, u32[]{:S(2)}, u32[]{:S(2)}) collective-permute-start(bf16[3072,128]{1,0:T(8,128)(2,1)} %collective-permute-done.13.refs_4_), channel_id=1, source_target_pairs={{0,14},{1,15},{2,0},{3,1},{4,2},{5,3},{6,4},{7,5},{8,6},{9,7},{10,... | collective-permute-start | bytes 2359304 | tf_op jit(solution)/shard_map/ppermute | solution.py:299
  123.6 34.0 %collective-permute-start.23 = (bf16[3072,128]{1,0:T(8,128)(2,1)}, bf16[3072,128]{1,0:T(8,128)(2,1)}, u32[]{:S(2)}, u32[]{:S(2)}) collective-permute-start(bf16[3072,128]{1,0:T(8,128)(2,1)} %collective-permute-done.21.refs_13_), channel_id=1, source_target_pairs={{0,14},{1,15},{2,0},{3,1},{4,2},{5,3},{6,4},{7,5},{8,6},{9,7},{10,... | collective-permute-start | bytes 2359304 | tf_op jit(solution)/shard_map/ppermute | solution.py:299
  123.7 37.3 %collective-permute-start.16 = (bf16[3072,128]{1,0:T(8,128)(2,1)}, bf16[3072,128]{1,0:T(8,128)(2,1)}, u32[]{:S(2)}, u32[]{:S(2)}) collective-permute-start(bf16[3072,128]{1,0:T(8,128)(2,1)} %collective-permute-done.14.refs_5_), channel_id=1, source_target_pairs={{0,2},{1,3},{2,4},{3,5},{4,6},{5,7},{6,8},{7,9},{8,10},{9,11},{10,... | collective-permute-start | bytes 2359304 | tf_op jit(solution)/shard_map/ppermute | solution.py:299
  141.6 33.6 %collective-permute-start.22 = (bf16[3072,128]{1,0:T(8,128)(2,1)}, bf16[3072,128]{1,0:T(8,128)(2,1)S(1)}, u32[]{:S(2)}, u32[]{:S(2)}) collective-permute-start(bf16[3072,128]{1,0:T(8,128)(2,1)} %collective-permute-done.20.refs_12_), channel_id=1, source_target_pairs={{0,2},{1,3},{2,4},{3,5},{4,6},{5,7},{6,8},{7,9},{8,10},{9,11},{10,... | collective-permute-start | bytes 2359304 | tf_op jit(solution)/shard_map/ppermute | solution.py:299
  141.6 33.6 %collective-permute-start.17 = (bf16[3072,128]{1,0:T(8,128)(2,1)}, bf16[3072,128]{1,0:T(8,128)(2,1)S(1)}, u32[]{:S(2)}, u32[]{:S(2)}) collective-permute-start(bf16[3072,128]{1,0:T(8,128)(2,1)} %collective-permute-done.15.refs_6_), channel_id=1, source_target_pairs={{0,14},{1,15},{2,0},{3,1},{4,2},{5,3},{6,4},{7,5},{8,6},{9,7},{10,... | collective-permute-start | bytes 2359304 | tf_op jit(solution)/shard_map/ppermute | solution.py:299
  157.6 33.7 %collective-permute-start.25 = (bf16[3072,128]{1,0:T(8,128)(2,1)}, bf16[3072,128]{1,0:T(8,128)(2,1)S(1)}, u32[]{:S(2)}, u32[]{:S(2)}) collective-permute-start(bf16[3072,128]{1,0:T(8,128)(2,1)} %collective-permute-done.23.refs_15_), channel_id=1, source_target_pairs={{0,14},{1,15},{2,0},{3,1},{4,2},{5,3},{6,4},{7,5},{8,6},{9,7},{10,... | collective-permute-start | bytes 2359304 | tf_op jit(solution)/shard_map/ppermute | solution.py:299
  161.1 31.0 %collective-permute-start.24 = (bf16[3072,128]{1,0:T(8,128)(2,1)}, bf16[3072,128]{1,0:T(8,128)(2,1)S(1)}, u32[]{:S(2)}, u32[]{:S(2)}) collective-permute-start(bf16[3072,128]{1,0:T(8,128)(2,1)} %collective-permute-done.16.refs_7_), channel_id=1, source_target_pairs={{0,2},{1,3},{2,4},{3,5},{4,6},{5,7},{6,8},{7,9},{8,10},{9,11},{10,... | collective-permute-start | bytes 2359304 | tf_op jit(solution)/shard_map/ppermute | solution.py:299
  161.1 3.4 %collective-permute-start.11 = (bf16[144,2048]{1,0:T(8,128)(2,1)S(1)}, bf16[144,2048]{1,0:T(8,128)(2,1)S(1)}, u32[]{:S(2)}, u32[]{:S(2)}) collective-permute-start(bf16[144,2048]{1,0:T(8,128)(2,1)S(1)} %pad_maximum_fusion.3.refs_0_), channel_id=1, source_target_pairs={{0,1},{1,0},{2,3},{3,2},{4,5},{5,4},{6,7},{7,6},{8,9},{9,8},{10,11... | collective-permute-start | bytes 1769480 | tf_op jit(solution)/shard_map/ppermute | solution.py:304
  198.1 2.4 %collective-permute-start.26 = (bf16[144,2048]{1,0:T(8,128)(2,1)S(1)}, bf16[144,2048]{1,0:T(8,128)(2,1)S(1)}, u32[]{:S(2)}, u32[]{:S(2)}) collective-permute-start(bf16[144,2048]{1,0:T(8,128)(2,1)S(1)} %get-tuple-element.8), channel_id=1, source_target_pairs={{0,1},{1,0},{2,3},{3,2},{4,5},{5,4},{6,7},{7,6},{8,9},{9,8},{10,11... | collective-permute-start | bytes 1769480 | tf_op jit(solution)/shard_map/ppermute | solution.py:304
  200.6 7.7 %copy-start.13 = (f32[64,2]{0,1:T(2,128)S(1)}, f32[64,2]{0,1:T(2,128)}, u32[]{:S(2)}) copy-start(f32[64,2]{0,1:T(2,128)} %param.30) | copy-start | bytes 1540
  201.5 18.3 %copy-start.1 = (f32[64,2048]{1,0:T(8,128)S(1)}, f32[64,2048]{1,0:T(8,128)}, u32[]{:S(2)}) copy-start(f32[64,2048]{1,0:T(8,128)} %copy-done) | copy-start | bytes 1572868
  201.5 18.2 %all-to-all-start.2 = ((bf16[16,144,128]{2,1,0:T(8,128)(2,1)}), bf16[16,144,128]{2,1,0:T(8,128)(2,1)S(1)}, u32[]{:S(2)}, u32[]{:S(2)}) async-start(bf16[16,144,128]{2,1,0:T(8,128)(2,1)} %pad_maximum_fusion.4), calls=%async_computation.2 | async-start | bytes 1179648 | tf_op jit(solution)/shard_map/all_to_all | solution.py:294

commit v2 on v1

--- a/solution.py
+++ b/solution.py
@@ -38,10 +38,12 @@
     ).astype(jnp.bfloat16)
 
 
-def attend_kernel(qs_ref, ks_ref, *refs, tq, tk, kb, parts):
+def attend_kernel(*refs, tq, tk, kb, parts):
+    me = lax.axis_index("sp")
+    my_y, my_x = me // SIDE, me % SIDE
     q_in, kv_in = refs[:parts], refs[parts : 2 * parts]
-    out_ref = refs[2 * parts]
-    q_buf, kv_buf, k_nat, v_aug, acc, peak, sems = refs[2 * parts + 1 :]
+    out_refs = refs[2 * parts : 3 * parts]
+    q_buf, kv_buf, k_nat, v_aug, acc, peak, out_buf, sems = refs[3 * parts :]
     span = kv_buf.shape[2]
     copies = []
     for i in range(parts):
@@ -65,13 +67,15 @@
 
     def q_tile(t, carry):
         i, h = t // per_q, t % per_q
-        q_start = qs_ref[t]
+        row = jnp.where(h == 0, my_y, SIDE - 1 - my_y)
+        q_start = (row * SIDE + (my_x + SIDE - i) % SIDE) * span + h * tq
         q = q_buf[i, :, pl.ds(pl.multiple_of(h * tq, tq), tq)]
         acc[...] = jnp.zeros_like(acc)
         peak[...] = jnp.full_like(peak, LOW)
 
         def k_tile(u, c):
-            k_start = ks_ref[u // per_k] + (u % per_k) * tk
+            k_row = (my_y + SIDE - u // per_k) % SIDE
+            k_start = (k_row * SIDE + my_x) * span + (u % per_k) * tk
 
             def score(r, masked):
                 keys = k_nat[pl.ds(pl.multiple_of(u * tk + r * kb, kb), kb), :]
@@ -124,18 +128,19 @@
             jnp.where(row == 1, mid.astype(jnp.float32), jnp.where(row == 2, lo.astype(jnp.float32), 0.0)),
         )
         cols = pl.ds(pl.multiple_of(h * tq, tq), tq)
-        out_ref[i, :VH, cols] = (acc[:VH, :] / safe).astype(jnp.bfloat16)
-        out_ref[i, VH:, cols] = stats.astype(jnp.bfloat16)
+        out_buf[i, :VH, cols] = (acc[:VH, :] / safe).astype(jnp.bfloat16)
+        out_buf[i, VH:, cols] = stats.astype(jnp.bfloat16)
         return carry
 
     lax.fori_loop(0, parts * per_q, q_tile, 0)
-
-
-def attend(q_parts, kv_parts, q_starts, k_starts, tq=512, tk=1024, kb=512):
+    for i in range(parts):
+        out_refs[i][...] = out_buf[i]
+
+
+def attend(q_parts, kv_parts, tq=512, tk=1024, kb=512):
     parts = len(q_parts)
     span = q_parts[0].shape[1]
     hbm = pl.BlockSpec(memory_space=pltpu.HBM)
-    smem = pl.BlockSpec(memory_space=pltpu.SMEM)
 
     def kernel(*refs):
         attend_kernel(*refs, tq=tq, tk=tk, kb=kb, parts=parts)
@@ -143,9 +148,9 @@
     work = parts * parts * span * span // 2
     return pl.pallas_call(
         kernel,
-        out_shape=jax.ShapeDtypeStruct((parts, VH + 16, span), jnp.bfloat16),
-        in_specs=[smem, smem] + [hbm] * (2 * parts),
-        out_specs=pl.BlockSpec(memory_space=pltpu.VMEM),
+        out_shape=[jax.ShapeDtypeStruct((VH + 16, span), jnp.bfloat16)] * parts,
+        in_specs=[hbm] * (2 * parts),
+        out_specs=[pl.BlockSpec(memory_space=pltpu.VMEM)] * parts,
         scratch_shapes=[
             pltpu.VMEM((parts, QK, span), jnp.bfloat16),
             pltpu.VMEM((parts, QK + VH, span), jnp.bfloat16),
@@ -153,6 +158,7 @@
             pltpu.VMEM((parts * span // tk, VH + 16, tk), jnp.bfloat16),
             pltpu.VMEM((VH + 16, tq), jnp.float32),
             pltpu.VMEM((8, tq), jnp.float32),
+            pltpu.VMEM((parts, VH + 16, span), jnp.bfloat16),
             pltpu.SemaphoreType.DMA((2 * parts,)),
         ],
         compiler_params=pltpu.CompilerParams(vmem_limit_bytes=60 * 1024 * 1024),
@@ -160,7 +166,7 @@
             flops=2 * work * (QK + VH), bytes_accessed=3 * 1024 * 1024, transcendentals=work
         ),
         name="attend",
-    )(q_starts, k_starts, *q_parts, *kv_parts)
+    )(*q_parts, *kv_parts)
 
 
 def expert_group(rows, w_buf, slots):
@@ -327,7 +333,6 @@
     half_len = shard_len // 2
     sp_count = lax.axis_size("sp")
     me = lax.axis_index("sp")
-    my_y, my_x = me // SIDE, me % SIDE
 
     gate, up, down = expert_gate[0], expert_up[0], expert_down[0]
     down = down.reshape(down.shape[0], D // LANES, LANES).transpose(1, 0, 2).reshape(-1, LANES)
@@ -373,23 +378,11 @@
     shifts = range(SIDE)
     kv_parts = [bundle] + [column_shift(bundle, k) for k in shifts[1:]]
     q_parts = [q_set] + [row_shift(q_set, k) for k in shifts[1:]]
-    k_starts = jnp.stack([((my_y - k) % SIDE * SIDE + my_x) * shard_len for k in shifts])
-    q_cols = [(my_x - k) % SIDE for k in shifts]
-    q_starts = jnp.stack(
-        sum(
-            [
-                [
-                    (my_y * SIDE + c) * shard_len,
-                    ((SIDE - 1 - my_y) * SIDE + c) * shard_len + half_len,
-                ]
-                for c in q_cols
-            ],
-            [],
-        )
-    )
-    partial = attend(q_parts, kv_parts, q_starts.astype(jnp.int32), k_starts.astype(jnp.int32))
+    partial = attend(q_parts, kv_parts)
     pieces = [partial[0]] + [row_shift(partial[k], -k) for k in shifts[1:]]
-    levels = [jnp.sum(p[VH : VH + 3].astype(jnp.float32), axis=0, keepdims=True) for p in pieces]
+    levels = [
+        sum(p[VH + j : VH + j + 1].astype(jnp.float32) for j in range(3)) for p in pieces
+    ]
     top = levels[0]
     for level in levels[1:]:
         top = jnp.maximum(top, level)

time: 222 us -> 216 us (0.973)
  waiting for transfers between devices: 107 us -> 104 us
  local copies, waits for them, and re-layouts: 9.89 us -> 7.44 us
    ppermute x6, waiting for transfers between devices: 15.9 us -> 12.9 us  [row_shift(): return lax.ppermute(value, 'sp', pairs)]
  transfers between devices with their start and end apart: 30 -> 30, of which waited for: 16 -> 17; matrix products, arithmetic and copies ran while one was open for 8% -> 7% of each run, Pallas kernels for 10% -> 10%
where the time goes in v2:
time: 216 us; the launch traced here: 215 us
  waiting for transfers between devices  104 us (48%)
  starting transfers between devices  60.3 us (28%)
  Pallas kernels  28 us (13%)
  other arithmetic  7.82 us (4%)
  local copies, waits for them, and re-layouts  7.44 us (3%)
  matrix products  6.69 us (3%)
    ppermute x14, waiting for transfers between devices, z_shift(): lax.ppermute(value, 'tp', [(t, (t + CORES * k) % count) for t in range(co...  46.8 us
    pallas_call x1, Pallas kernels, attend(): pl.pallas_call(kernel, out_shape=[jax.ShapeDtypeStruct((VH + 16, span), j...  22 us
    ppermute x14, starting transfers between devices, z_shift(): lax.ppermute(value, 'tp', [(t, (t + CORES * k) % count) for t in range(co...  21.1 us
    all_to_all x2, waiting for transfers between devices, expert_exchange(): return lax.all_to_all(wire, 'sp', split_axis=0, concat_axis=0, tiled=True)  19.9 us
    ppermute x2, waiting for transfers between devices, row_swap(): return lax.ppermute(value, 'sp', pairs)  15.6 us
    all_to_all x2, starting transfers between devices, expert_exchange(): return lax.all_to_all(wire, 'sp', split_axis=0, concat_axis=0, tiled=True)  13.1 us
    ppermute x6, waiting for transfers between devices, row_shift(): return lax.ppermute(value, 'sp', pairs)  12.9 us
    all_to_all x1, starting transfers between devices, shards(): lax.all_to_all(attended.T, 'tp', split_axis=0, concat_axis=1, tiled=True)  6.73 us
  transfers between devices with their start and end apart: 30, of which 17 were waited for; matrix products, arithmetic and copies ran while one was open for 7% of the time, Pallas kernels for 10%

profile of v2, /device:TPU:1, one launch (start us, length us, event | category | flops | bytes accessed | tf_op | source)
XLA Modules:
  0.0 215.4 jit_solution(7051171362010102041)
XLA Ops:
  0.0 1.5 fusion.1
  1.6 2.0 convolution_convert_fusion.1
  4.1 0.3 fusion.37
  4.4 2.2 %collective-permute-start.4 = (bf16[160,1024]{1,0:T(8,128)(2,1)S(1)}, bf16[160,1024]{1,0:T(8,128)(2,1)}, u32[]{:S(2)}, u32[]{:S(2)}) collective-permute-start(bf16[160,1024]{1,0:T(8,128)(2,1)S(1)} %pad_maximum_fusion.5.refs_4_), channel_id=1, source_target_pairs={{0,64},{16,80},{32,96},{48,112},{64,128},{80,144},{96,160},{112,17... | collective-permute-start | bytes 983048 | tf_op jit(solution)/shard_map/ppermute | solution.py:289
  6.6 2.6 %collective-permute-start.5 = (bf16[160,1024]{1,0:T(8,128)(2,1)S(1)}, bf16[160,1024]{1,0:T(8,128)(2,1)}, u32[]{:S(2)}, u32[]{:S(2)}) collective-permute-start(bf16[160,1024]{1,0:T(8,128)(2,1)S(1)} %pad_maximum_fusion.5.refs_4_), channel_id=1, source_target_pairs={{0,128},{16,144},{32,160},{48,176},{64,192},{80,208},{96,224},{112... | collective-permute-start | bytes 983048 | tf_op jit(solution)/shard_map/ppermute | solution.py:289
  9.3 1.1 collective-permute-start.6
  10.7 0.1 eq.14
  11.1 13.9 %collective-permute-done = bf16[96,512]{1,0:T(8,128)(2,1)S(1)} collective-permute-done((bf16[96,512]{1,0:T(8,128)(2,1)S(1)}, bf16[96,512]{1,0:T(8,128)(2,1)S(1)}, u32[]{:S(2)}, u32[]{:S(2)}) %collective-permute-start) | collective-permute-done | bytes 98336 | tf_op jit(solution)/shard_map/ppermute | solution.py:296
  25.1 1.3 collective-permute-start.1
  26.4 2.5 %collective-permute-start.2 = (bf16[96,1024]{1,0:T(8,128)(2,1)S(1)}, bf16[96,1024]{1,0:T(8,128)(2,1)S(1)}, u32[]{:S(2)}, u32[]{:S(2)}) collective-permute-start(bf16[96,1024]{1,0:T(8,128)(2,1)S(1)} %pad_maximum_fusion.7.refs_0_), channel_id=1, source_target_pairs={{0,32},{16,48},{32,0},{48,16},{64,96},{80,112},{96,64},{112,80},{1... | collective-permute-start | bytes 589832 | tf_op jit(solution)/shard_map/ppermute | solution.py:282
  28.9 3.0 %collective-permute-done.1.refs_1_ = bf16[96,1024]{1,0:T(8,128)(2,1)S(1)} collective-permute-done((bf16[96,1024]{1,0:T(8,128)(2,1)S(1)}, bf16[96,1024]{1,0:T(8,128)(2,1)S(1)}, u32[]{:S(2)}, u32[]{:S(2)}) %collective-permute-start.1) | collective-permute-done | bytes 196640 | tf_op jit(solution)/shard_map/ppermute | solution.py:282
  32.0 1.3 collective-permute-start.3
  33.3 3.9 %collective-permute-done.2.refs_2_ = bf16[96,1024]{1,0:T(8,128)(2,1)S(1)} collective-permute-done((bf16[96,1024]{1,0:T(8,128)(2,1)S(1)}, bf16[96,1024]{1,0:T(8,128)(2,1)S(1)}, u32[]{:S(2)}, u32[]{:S(2)}) %collective-permute-start.2) | collective-permute-done | bytes 196640 | tf_op jit(solution)/shard_map/ppermute | solution.py:282
  37.2 5.6 %collective-permute-start.19 = (bf16[3072,128]{1,0:T(8,128)(2,1)S(1)}, bf16[3072,128]{1,0:T(8,128)(2,1)S(1)}, u32[]{:S(2)}, u32[]{:S(2)}) collective-permute-start(bf16[3072,128]{1,0:T(8,128)(2,1)S(1)} %pad_maximum_fusion.1.refs_9_), channel_id=1, source_target_pairs={{0,14},{1,15},{2,0},{3,1},{4,2},{5,3},{6,4},{7,5},{8,6},{9,7},{10,... | collective-permute-start | bytes 2359304 | tf_op jit(solution)/shard_map/ppermute | solution.py:305
  42.8 22.0 %attend.1 = (bf16[80,1024]{1,0:T(8,128)(2,1)}, bf16[80,1024]{1,0:T(8,128)(2,1)}, bf16[80,1024]{1,0:T(8,128)(2,1)}, bf16[80,1024]{1,0:T(8,128)(2,1)}) custom-call(bf16[96,1024]{1,0:T(8,128)(2,1)} %copy-done.8, bf16[96,1024]{1,0:T(8,128)(2,1)} %copy-done.16, bf16[96,1024]{1,0:T(8,128)(2,1)} %copy-done.17, bf16[96,1024]{1,0:T(8,128)(2,1)} %collective-permute-done.3.refs_3_, ...), custom_call_target="tpu_custom_call" | custom-call | flops 2684354560 | bytes 3145728 | tf_op jit(solution)/shard_map/attend/pallas_call | solution.py:149
  65.0 1.4 collective-permute-start.9
  66.4 0.2 reduce_window_sum.11
  66.6 2.6 %collective-permute-done.7 = bf16[80,1024]{1,0:T(8,128)(2,1)S(1)} collective-permute-done((bf16[80,1024]{1,0:T(8,128)(2,1)}, bf16[80,1024]{1,0:T(8,128)(2,1)S(1)}, u32[]{:S(2)}, u32[]{:S(2)}) %collective-permute-start.7) | collective-permute-done | bytes 163872 | tf_op jit(solution)/shard_map/ppermute | solution.py:282
  69.2 1.8 collective-permute-done.8
  71.0 2.7 %collective-permute-start.13 = (bf16[3072,128]{1,0:T(8,128)(2,1)S(1)}, bf16[3072,128]{1,0:T(8,128)(2,1)}, u32[]{:S(2)}, u32[]{:S(2)}) collective-permute-start(bf16[3072,128]{1,0:T(8,128)(2,1)S(1)} %pad_maximum_fusion.refs_2_), channel_id=1, source_target_pairs={{0,14},{1,15},{2,0},{3,1},{4,2},{5,3},{6,4},{7,5},{8,6},{9,7},{10,... | collective-permute-start | bytes 2359304 | tf_op jit(solution)/shard_map/ppermute | solution.py:305
  73.7 1.6 collective-permute-done.9
  75.3 0.9 maximum_maximum_fusion
  76.2 1.2 divide_convert_fusion
  77.4 4.2 %collective-permute-start.10 = (bf16[64,512]{1,0:T(8,128)(2,1)S(1)}, bf16[64,512]{1,0:T(8,128)(2,1)S(1)}, u32[]{:S(2)}, u32[]{:S(2)}) collective-permute-start(bf16[64,512]{1,0:T(8,128)(2,1)S(1)} %get-tuple-element.38), channel_id=1, source_target_pairs={{0,192},{16,208},{32,224},{48,240},{64,128},{80,144},{96,160},{112... | collective-permute-start | bytes 196616 | tf_op jit(solution)/shard_map/ppermute | solution.py:296
  81.6 0.2 select_reduce_fusion.1
  81.8 0.1 reduce_sum.82
  82.0 1.7 collective-permute-done.10
  83.7 0.2 copy.57
  83.9 0.9 reshape.130
  84.8 6.7 %all-to-all-start = ((bf16[16,2,2048]{2,1,0:T(2,128)(2,1)}), bf16[16,2,2048]{2,1,0:T(2,128)(2,1)S(1)}, u32[]{:S(2)}, u32[]{:S(2)}) async-start(bf16[16,2,2048]{2,1,0:T(2,128)(2,1)} %reshape.130), calls=%async_computation | async-start | bytes 262144 | tf_op jit(solution)/shard_map/all_to_all | solution.py:395
  91.5 0.7 fusion.40
  92.2 2.6 %collective-permute-start.21 = (bf16[3072,128]{1,0:T(8,128)(2,1)S(1)}, bf16[3072,128]{1,0:T(8,128)(2,1)}, u32[]{:S(2)}, u32[]{:S(2)}) collective-permute-start(bf16[3072,128]{1,0:T(8,128)(2,1)S(1)} %collective-permute-done.19.refs_11_), channel_id=1, source_target_pairs={{0,14},{1,15},{2,0},{3,1},{4,2},{5,3},{6,4},{7,5},{8,6},{9,7},{10,... | collective-permute-start | bytes 2359304 | tf_op jit(solution)/shard_map/ppermute | solution.py:305
  94.8 6.0 %all-to-all-done = bf16[16,2,2048]{2,1,0:T(2,128)(2,1)S(1)} async-done(((bf16[16,2,2048]{2,1,0:T(2,128)(2,1)}), bf16[16,2,2048]{2,1,0:T(2,128)(2,1)S(1)}, u32[]{:S(2)}, u32[]{:S(2)}) %all-to-all-start) | async-done | bytes 131104 | tf_op jit(solution)/shard_map/all_to_all | solution.py:395
  100.8 0.2 reshape.131
  101.0 0.2 fusion.10
  101.2 1.1 copy.52
  102.3 1.2 reshape.129
  103.5 3.2 %multiply_reduce_fusion = (f32[64]{0:T(128)S(1)}, f32[64,2048]{1,0:T(8,128)S(1)}) fusion(bf16[1024,2048]{1,0:T(8,128)(2,1)} %param.26, f32[64,1024]{1,0:T(8,128)S(1)} %reshape.129, f32[1024]{0:T(1024)S(1)} %copy-done.11, f32[64]{0:T(128)S(1)} %add_rsqrt_fusion.4, bf16[64,2048]{1,0:T(8,128)(2,1)} %param.27), kind=kOutput, calls=%fused_computation.29 | convolution fusion | flops 269156288 | bytes 5247488 | tf_op jit(solution)/shard_map/dot_general | solution.py:398
  106.8 0.8 copy-done
  107.7 0.4 convolution_convert_fusion
  108.1 0.9 pad_maximum_fusion.2
  109.0 6.4 %all-to-all-start.1 = ((bf16[16,144,128]{2,1,0:T(8,128)(2,1)}), bf16[16,144,128]{2,1,0:T(8,128)(2,1)}, u32[]{:S(2)}, u32[]{:S(2)}) async-start(bf16[16,144,128]{2,1,0:T(8,128)(2,1)} %pad_maximum_fusion.2), calls=%async_computation.1 | async-start | bytes 1179648 | tf_op jit(solution)/shard_map/all_to_all | solution.py:300
  115.5 2.7 %collective-permute-start.15 = (bf16[3072,128]{1,0:T(8,128)(2,1)}, bf16[3072,128]{1,0:T(8,128)(2,1)}, u32[]{:S(2)}, u32[]{:S(2)}) collective-permute-start(bf16[3072,128]{1,0:T(8,128)(2,1)} %collective-permute-done.13.refs_4_), channel_id=1, source_target_pairs={{0,14},{1,15},{2,0},{3,1},{4,2},{5,3},{6,4},{7,5},{8,6},{9,7},{10,... | collective-permute-start | bytes 2359304 | tf_op jit(solution)/shard_map/ppermute | solution.py:305
  118.3 1.4 collective-permute-start.16
  119.6 8.6 %all-to-all-done.1 = bf16[16,144,128]{2,1,0:T(8,128)(2,1)} async-done(((bf16[16,144,128]{2,1,0:T(8,128)(2,1)}), bf16[16,144,128]{2,1,0:T(8,128)(2,1)}, u32[]{:S(2)}, u32[]{:S(2)}) %all-to-all-start.1) | async-done | bytes 589856 | tf_op jit(solution)/shard_map/all_to_all | solution.py:300
  128.3 0.8 slice.189
  129.1 1.1 slice_bitcast_fusion.2
  130.2 5.9 %collective-permute-done.20.refs_12_ = bf16[3072,128]{1,0:T(8,128)(2,1)} collective-permute-done((bf16[3072,128]{1,0:T(8,128)(2,1)S(1)}, bf16[3072,128]{1,0:T(8,128)(2,1)}, u32[]{:S(2)}, u32[]{:S(2)}) %collective-permute-start.20) | collective-permute-done | bytes 786464 | tf_op jit(solution)/shard_map/ppermute | solution.py:305
  136.1 2.7 %collective-permute-start.17 = (bf16[3072,128]{1,0:T(8,128)(2,1)}, bf16[3072,128]{1,0:T(8,128)(2,1)S(1)}, u32[]{:S(2)}, u32[]{:S(2)}) collective-permute-start(bf16[3072,128]{1,0:T(8,128)(2,1)} %collective-permute-done.15.refs_6_), channel_id=1, source_target_pairs={{0,14},{1,15},{2,0},{3,1},{4,2},{5,3},{6,4},{7,5},{8,6},{9,7},{10,... | collective-permute-start | bytes 2359304 | tf_op jit(solution)/shard_map/ppermute | solution.py:305
  138.8 13.4 %collective-permute-done.23.refs_15_ = bf16[3072,128]{1,0:T(8,128)(2,1)} collective-permute-done((bf16[3072,128]{1,0:T(8,128)(2,1)}, bf16[3072,128]{1,0:T(8,128)(2,1)}, u32[]{:S(2)}, u32[]{:S(2)}) %collective-permute-start.23) | collective-permute-done | bytes 786464 | tf_op jit(solution)/shard_map/ppermute | solution.py:305
  152.2 3.4 %collective-permute-start.25 = (bf16[3072,128]{1,0:T(8,128)(2,1)}, bf16[3072,128]{1,0:T(8,128)(2,1)S(1)}, u32[]{:S(2)}, u32[]{:S(2)}) collective-permute-start(bf16[3072,128]{1,0:T(8,128)(2,1)} %collective-permute-done.23.refs_15_), channel_id=1, source_target_pairs={{0,14},{1,15},{2,0},{3,1},{4,2},{5,3},{6,4},{7,5},{8,6},{9,7},{10,... | collective-permute-start | bytes 2359304 | tf_op jit(solution)/shard_map/ppermute | solution.py:305
  155.7 1.8 collective-permute-start.11
  157.4 1.6 collective-permute-done.11.refs_1_
  159.1 10.6 %collective-permute-done.22.refs_14_ = bf16[3072,128]{1,0:T(8,128)(2,1)S(1)} collective-permute-done((bf16[3072,128]{1,0:T(8,128)(2,1)}, bf16[3072,128]{1,0:T(8,128)(2,1)S(1)}, u32[]{:S(2)}, u32[]{:S(2)}) %collective-permute-start.22) | collective-permute-done | bytes 786464 | tf_op jit(solution)/shard_map/ppermute | solution.py:305
  169.7 16.2 %collective-permute-done.25.refs_17_ = bf16[3072,128]{1,0:T(8,128)(2,1)S(1)} collective-permute-done((bf16[3072,128]{1,0:T(8,128)(2,1)}, bf16[3072,128]{1,0:T(8,128)(2,1)S(1)}, u32[]{:S(2)}, u32[]{:S(2)}) %collective-permute-start.25) | collective-permute-done | bytes 786464 | tf_op jit(solution)/shard_map/ppermute | solution.py:305
  185.9 0.7 collective-permute-done.24.refs_16_
  186.6 6.0 %expert_ffn.1 = (bf16[144,2048]{1,0:T(8,128)(2,1)S(1)}, bf16[144,2048]{1,0:T(8,128)(2,1)S(1)}) custom-call(bf16[144,2048]{1,0:T(8,128)(2,1)S(1)} %pad_maximum_fusion.3.refs_0_, bf16[144,2048]{1,0:T(8,128)(2,1)S(1)} %collective-permute-done.11.refs_1_, bf16[3072,128]{1,0:T(8,128)(2,1)S(1)} %pad_maximum_fusion.refs_2_, ...), custom_call_target="tpu_custom_call" | custom-call | flops 3623878656 | bytes 12582912 | tf_op jit(solution)/shard_map/expert_ffn/pallas_call | solution.py:225
  192.6 0.7 collective-permute-start.26
  193.3 1.6 collective-permute-done.26
  195.0 0.1 add_convert_fusion
  195.2 0.9 pad_maximum_fusion.4
  196.1 6.7 %all-to-all-start.2 = ((bf16[16,144,128]{2,1,0:T(8,128)(2,1)}), bf16[16,144,128]{2,1,0:T(8,128)(2,1)S(1)}, u32[]{:S(2)}, u32[]{:S(2)}) async-start(bf16[16,144,128]{2,1,0:T(8,128)(2,1)} %pad_maximum_fusion.4), calls=%async_computation.2 | async-start | bytes 1179648 | tf_op jit(solution)/shard_map/all_to_all | solution.py:300
  202.9 11.3 %all-to-all-done.2 = bf16[16,144,128]{2,1,0:T(8,128)(2,1)S(1)} async-done(((bf16[16,144,128]{2,1,0:T(8,128)(2,1)}), bf16[16,144,128]{2,1,0:T(8,128)(2,1)S(1)}, u32[]{:S(2)}, u32[]{:S(2)}) %all-to-all-start.2) | async-done | bytes 589856 | tf_op jit(solution)/shard_map/all_to_all | solution.py:300
  214.3 1.1 fusion
  (101 shorter events, 2.1 us)
Async XLA Ops:
  1.5 2.1 copy-start.7
  1.5 2.2 copy-start.2
  1.5 2.2 %copy-start.14 = (f32[96]{0:T(128)S(1)}, f32[96]{0:T(128)}, u32[]{:S(2)}) copy-start(f32[96]{0:T(128)} %param.24) | copy-start | bytes 1156
  1.6 2.4 %copy-start.15 = (f32[96]{0:T(128)S(1)}, f32[96]{0:T(128)}, u32[]{:S(2)}) copy-start(f32[96]{0:T(128)} %param.23) | copy-start | bytes 1156
  3.9 6.6 %copy-start.4 = (bf16[1,2048,128]{2,1,0:T(8,128)(2,1)S(1)}, bf16[1,2048,128]{2,1,0:T(8,128)(2,1)}, u32[]{:S(2)}) copy-start(bf16[1,2048,128]{2,1,0:T(8,128)(2,1)} %param.32) | copy-start | bytes 1572868
  4.0 6.5 %copy-start.12 = (s32[64,2]{0,1:T(2,128)S(1)}, s32[64,2]{0,1:T(2,128)}, u32[]{:S(2)}) copy-start(s32[64,2]{0,1:T(2,128)} %param.29) | copy-start | bytes 1540
  4.0 6.7 %copy-start.5 = (bf16[1,128,2048]{2,1,0:T(8,128)(2,1)S(1)}, bf16[1,128,2048]{2,1,0:T(8,128)(2,1)}, u32[]{:S(2)}) copy-start(bf16[1,128,2048]{2,1,0:T(8,128)(2,1)} %param.33) | copy-start | bytes 1572868
  4.4 6.5 %copy-start.6 = (bf16[160,1024]{1,0:T(8,128)(2,1)}, bf16[160,1024]{1,0:T(8,128)(2,1)S(1)}, u32[]{:S(2)}) copy-start(bf16[160,1024]{1,0:T(8,128)(2,1)S(1)} %pad_maximum_fusion.5.refs_4_) | copy-start | bytes 983044
  4.4 38.3 %collective-permute-start.4 = (bf16[160,1024]{1,0:T(8,128)(2,1)S(1)}, bf16[160,1024]{1,0:T(8,128)(2,1)}, u32[]{:S(2)}, u32[]{:S(2)}) collective-permute-start(bf16[160,1024]{1,0:T(8,128)(2,1)S(1)} %pad_maximum_fusion.5.refs_4_), channel_id=1, source_target_pairs={{0,64},{16,80},{32,96},{48,112},{64,128},{80,144},{96,160},{112,17... | collective-permute-start | bytes 983048 | tf_op jit(solution)/shard_map/ppermute | solution.py:289
  6.6 36.1 %collective-permute-start.5 = (bf16[160,1024]{1,0:T(8,128)(2,1)S(1)}, bf16[160,1024]{1,0:T(8,128)(2,1)}, u32[]{:S(2)}, u32[]{:S(2)}) collective-permute-start(bf16[160,1024]{1,0:T(8,128)(2,1)S(1)} %pad_maximum_fusion.5.refs_4_), channel_id=1, source_target_pairs={{0,128},{16,144},{32,160},{48,176},{64,192},{80,208},{96,224},{112... | collective-permute-start | bytes 983048 | tf_op jit(solution)/shard_map/ppermute | solution.py:289
  9.3 33.5 %collective-permute-start.6 = (bf16[160,1024]{1,0:T(8,128)(2,1)S(1)}, bf16[160,1024]{1,0:T(8,128)(2,1)}, u32[]{:S(2)}, u32[]{:S(2)}) collective-permute-start(bf16[160,1024]{1,0:T(8,128)(2,1)S(1)} %pad_maximum_fusion.5.refs_4_), channel_id=1, source_target_pairs={{0,192},{16,208},{32,224},{48,240},{64,0},{80,16},{96,32},{112,48}... | collective-permute-start | bytes 983048 | tf_op jit(solution)/shard_map/ppermute | solution.py:289
  10.4 14.6 %collective-permute-start = (bf16[96,512]{1,0:T(8,128)(2,1)S(1)}, bf16[96,512]{1,0:T(8,128)(2,1)S(1)}, u32[]{:S(2)}, u32[]{:S(2)}) collective-permute-start(bf16[96,512]{1,0:T(8,128)(2,1)S(1)} %get-tuple-element.36), channel_id=1, source_target_pairs={{0,192},{16,208},{32,224},{48,240},{64,128},{80,144},{96,160},{112... | collective-permute-start | bytes 294920 | tf_op jit(solution)/shard_map/ppermute | solution.py:296
  10.9 22.3 %copy-start.3 = (bf16[1,2048,128]{2,1,0:T(8,128)(2,1)S(1)}, bf16[1,2048,128]{2,1,0:T(8,128)(2,1)}, u32[]{:S(2)}) copy-start(bf16[1,2048,128]{2,1,0:T(8,128)(2,1)} %param.31) | copy-start | bytes 1572868
  25.0 8.3 %copy-start.8 = (bf16[96,1024]{1,0:T(8,128)(2,1)}, bf16[96,1024]{1,0:T(8,128)(2,1)S(1)}, u32[]{:S(2)}) copy-start(bf16[96,1024]{1,0:T(8,128)(2,1)S(1)} %pad_maximum_fusion.7.refs_0_) | copy-start | bytes 589828
  25.1 6.9 %collective-permute-start.1 = (bf16[96,1024]{1,0:T(8,128)(2,1)S(1)}, bf16[96,1024]{1,0:T(8,128)(2,1)S(1)}, u32[]{:S(2)}, u32[]{:S(2)}) collective-permute-start(bf16[96,1024]{1,0:T(8,128)(2,1)S(1)} %pad_maximum_fusion.7.refs_0_), channel_id=1, source_target_pairs={{0,16},{16,32},{32,48},{48,0},{64,80},{80,96},{96,112},{112,64},{1... | collective-permute-start | bytes 589832 | tf_op jit(solution)/shard_map/ppermute | solution.py:282
  26.4 10.8 %collective-permute-start.2 = (bf16[96,1024]{1,0:T(8,128)(2,1)S(1)}, bf16[96,1024]{1,0:T(8,128)(2,1)S(1)}, u32[]{:S(2)}, u32[]{:S(2)}) collective-permute-start(bf16[96,1024]{1,0:T(8,128)(2,1)S(1)} %pad_maximum_fusion.7.refs_0_), channel_id=1, source_target_pairs={{0,32},{16,48},{32,0},{48,16},{64,96},{80,112},{96,64},{112,80},{1... | collective-permute-start | bytes 589832 | tf_op jit(solution)/shard_map/ppermute | solution.py:282
  32.0 10.8 %copy-start.16 = (bf16[96,1024]{1,0:T(8,128)(2,1)}, bf16[96,1024]{1,0:T(8,128)(2,1)S(1)}, u32[]{:S(2)}) copy-start(bf16[96,1024]{1,0:T(8,128)(2,1)S(1)} %collective-permute-done.1.refs_1_) | copy-start | bytes 589828
  32.0 10.8 %collective-permute-start.3 = (bf16[96,1024]{1,0:T(8,128)(2,1)S(1)}, bf16[96,1024]{1,0:T(8,128)(2,1)}, u32[]{:S(2)}, u32[]{:S(2)}) collective-permute-start(bf16[96,1024]{1,0:T(8,128)(2,1)S(1)} %pad_maximum_fusion.7.refs_0_), channel_id=1, source_target_pairs={{0,48},{16,0},{32,16},{48,32},{64,112},{80,64},{96,80},{112,96},{1... | collective-permute-start | bytes 589832 | tf_op jit(solution)/shard_map/ppermute | solution.py:282
  37.2 5.6 %copy-start.17 = (bf16[96,1024]{1,0:T(8,128)(2,1)}, bf16[96,1024]{1,0:T(8,128)(2,1)S(1)}, u32[]{:S(2)}) copy-start(bf16[96,1024]{1,0:T(8,128)(2,1)S(1)} %collective-permute-done.2.refs_2_) | copy-start | bytes 589828
  37.2 55.1 %collective-permute-start.19 = (bf16[3072,128]{1,0:T(8,128)(2,1)S(1)}, bf16[3072,128]{1,0:T(8,128)(2,1)S(1)}, u32[]{:S(2)}, u32[]{:S(2)}) collective-permute-start(bf16[3072,128]{1,0:T(8,128)(2,1)S(1)} %pad_maximum_fusion.1.refs_9_), channel_id=1, source_target_pairs={{0,14},{1,15},{2,0},{3,1},{4,2},{5,3},{6,4},{7,5},{8,6},{9,7},{10,... | collective-permute-start | bytes 2359304 | tf_op jit(solution)/shard_map/ppermute | solution.py:305
  42.7 72.7 %collective-permute-start.18 = (bf16[3072,128]{1,0:T(8,128)(2,1)S(1)}, bf16[3072,128]{1,0:T(8,128)(2,1)S(1)}, u32[]{:S(2)}, u32[]{:S(2)}) collective-permute-start(bf16[3072,128]{1,0:T(8,128)(2,1)S(1)} %pad_maximum_fusion.1.refs_9_), channel_id=1, source_target_pairs={{0,2},{1,3},{2,4},{3,5},{4,6},{5,7},{6,8},{7,9},{8,10},{9,11},{10,... | collective-permute-start | bytes 2359304 | tf_op jit(solution)/shard_map/ppermute | solution.py:305
  64.8 4.5 %collective-permute-start.7 = (bf16[80,1024]{1,0:T(8,128)(2,1)}, bf16[80,1024]{1,0:T(8,128)(2,1)S(1)}, u32[]{:S(2)}, u32[]{:S(2)}) collective-permute-start(bf16[80,1024]{1,0:T(8,128)(2,1)} %get-tuple-element.12), channel_id=1, source_target_pairs={{0,48},{16,0},{32,16},{48,32},{64,112},{80,64},{96,80},{112,96},{1... | collective-permute-start | bytes 491528 | tf_op jit(solution)/shard_map/ppermute | solution.py:282
  64.9 6.2 %collective-permute-start.8 = (bf16[80,1024]{1,0:T(8,128)(2,1)}, bf16[80,1024]{1,0:T(8,128)(2,1)}, u32[]{:S(2)}, u32[]{:S(2)}) collective-permute-start(bf16[80,1024]{1,0:T(8,128)(2,1)} %get-tuple-element.13), channel_id=1, source_target_pairs={{0,32},{16,48},{32,0},{48,16},{64,96},{80,112},{96,64},{112,80},{1... | collective-permute-start | bytes 491528 | tf_op jit(solution)/shard_map/ppermute | solution.py:282
  65.0 10.3 %collective-permute-start.9 = (bf16[80,1024]{1,0:T(8,128)(2,1)}, bf16[80,1024]{1,0:T(8,128)(2,1)}, u32[]{:S(2)}, u32[]{:S(2)}) collective-permute-start(bf16[80,1024]{1,0:T(8,128)(2,1)} %get-tuple-element.14), channel_id=1, source_target_pairs={{0,16},{16,32},{32,48},{48,0},{64,80},{80,96},{96,112},{112,64},{1... | collective-permute-start | bytes 491528 | tf_op jit(solution)/shard_map/ppermute | solution.py:282
  69.2 25.6 %collective-permute-start.12 = (bf16[3072,128]{1,0:T(8,128)(2,1)S(1)}, bf16[3072,128]{1,0:T(8,128)(2,1)}, u32[]{:S(2)}, u32[]{:S(2)}) collective-permute-start(bf16[3072,128]{1,0:T(8,128)(2,1)S(1)} %pad_maximum_fusion.refs_2_), channel_id=1, source_target_pairs={{0,2},{1,3},{2,4},{3,5},{4,6},{5,7},{6,8},{7,9},{8,10},{9,11},{10,... | collective-permute-start | bytes 2359304 | tf_op jit(solution)/shard_map/ppermute | solution.py:305
  71.0 44.5 %collective-permute-start.13 = (bf16[3072,128]{1,0:T(8,128)(2,1)S(1)}, bf16[3072,128]{1,0:T(8,128)(2,1)}, u32[]{:S(2)}, u32[]{:S(2)}) collective-permute-start(bf16[3072,128]{1,0:T(8,128)(2,1)S(1)} %pad_maximum_fusion.refs_2_), channel_id=1, source_target_pairs={{0,14},{1,15},{2,0},{3,1},{4,2},{5,3},{6,4},{7,5},{8,6},{9,7},{10,... | collective-permute-start | bytes 2359304 | tf_op jit(solution)/shard_map/ppermute | solution.py:305
  77.4 6.3 %collective-permute-start.10 = (bf16[64,512]{1,0:T(8,128)(2,1)S(1)}, bf16[64,512]{1,0:T(8,128)(2,1)S(1)}, u32[]{:S(2)}, u32[]{:S(2)}) collective-permute-start(bf16[64,512]{1,0:T(8,128)(2,1)S(1)} %get-tuple-element.38), channel_id=1, source_target_pairs={{0,192},{16,208},{32,224},{48,240},{64,128},{80,144},{96,160},{112... | collective-permute-start | bytes 196616 | tf_op jit(solution)/shard_map/ppermute | solution.py:296
  84.8 16.0 %all-to-all-start = ((bf16[16,2,2048]{2,1,0:T(2,128)(2,1)}), bf16[16,2,2048]{2,1,0:T(2,128)(2,1)S(1)}, u32[]{:S(2)}, u32[]{:S(2)}) async-start(bf16[16,2,2048]{2,1,0:T(2,128)(2,1)} %reshape.130), calls=%async_computation | async-start | bytes 262144 | tf_op jit(solution)/shard_map/all_to_all | solution.py:395
  92.2 11.3 %copy-start.11 = (f32[1024]{0:T(1024)S(1)}, f32[1024]{0:T(1024)}, u32[]{:S(2)}) copy-start(f32[1024]{0:T(1024)} %param.25) | copy-start | bytes 12292
  92.2 25.9 %collective-permute-start.21 = (bf16[3072,128]{1,0:T(8,128)(2,1)S(1)}, bf16[3072,128]{1,0:T(8,128)(2,1)}, u32[]{:S(2)}, u32[]{:S(2)}) collective-permute-start(bf16[3072,128]{1,0:T(8,128)(2,1)S(1)} %collective-permute-done.19.refs_11_), channel_id=1, source_target_pairs={{0,14},{1,15},{2,0},{3,1},{4,2},{5,3},{6,4},{7,5},{8,6},{9,7},{10,... | collective-permute-start | bytes 2359304 | tf_op jit(solution)/shard_map/ppermute | solution.py:305
  94.8 23.5 %collective-permute-start.14 = (bf16[3072,128]{1,0:T(8,128)(2,1)}, bf16[3072,128]{1,0:T(8,128)(2,1)}, u32[]{:S(2)}, u32[]{:S(2)}) collective-permute-start(bf16[3072,128]{1,0:T(8,128)(2,1)} %collective-permute-done.12.refs_3_), channel_id=1, source_target_pairs={{0,2},{1,3},{2,4},{3,5},{4,6},{5,7},{6,8},{7,9},{8,10},{9,11},{10,... | collective-permute-start | bytes 2359304 | tf_op jit(solution)/shard_map/ppermute | solution.py:305
  103.5 4.1 %copy-start.9 = (bf16[64,144]{1,0:T(8,128)(2,1)S(1)}, bf16[64,144]{1,0:T(8,128)(2,1)}, u32[]{:S(2)}) copy-start(bf16[64,144]{1,0:T(8,128)(2,1)} %fusion.40) | copy-start | bytes 55300
  103.5 4.1 %copy-start.10 = (f32[2048]{0:T(1024)S(1)}, f32[2048]{0:T(1024)}, u32[]{:S(2)}) copy-start(f32[2048]{0:T(1024)} %param.28) | copy-start | bytes 24580
  106.8 0.9 copy-start
  109.0 19.3 %all-to-all-start.1 = ((bf16[16,144,128]{2,1,0:T(8,128)(2,1)}), bf16[16,144,128]{2,1,0:T(8,128)(2,1)}, u32[]{:S(2)}, u32[]{:S(2)}) async-start(bf16[16,144,128]{2,1,0:T(8,128)(2,1)} %pad_maximum_fusion.2), calls=%async_computation.1 | async-start | bytes 1179648 | tf_op jit(solution)/shard_map/all_to_all | solution.py:300
  115.4 20.7 %collective-permute-start.20 = (bf16[3072,128]{1,0:T(8,128)(2,1)S(1)}, bf16[3072,128]{1,0:T(8,128)(2,1)}, u32[]{:S(2)}, u32[]{:S(2)}) collective-permute-start(bf16[3072,128]{1,0:T(8,128)(2,1)S(1)} %collective-permute-done.18.refs_10_), channel_id=1, source_target_pairs={{0,2},{1,3},{2,4},{3,5},{4,6},{5,7},{6,8},{7,9},{8,10},{9,11},{10,... | collective-permute-start | bytes 2359304 | tf_op jit(solution)/shard_map/ppermute | solution.py:305
  115.5 20.6 %collective-permute-start.15 = (bf16[3072,128]{1,0:T(8,128)(2,1)}, bf16[3072,128]{1,0:T(8,128)(2,1)}, u32[]{:S(2)}, u32[]{:S(2)}) collective-permute-start(bf16[3072,128]{1,0:T(8,128)(2,1)} %collective-permute-done.13.refs_4_), channel_id=1, source_target_pairs={{0,14},{1,15},{2,0},{3,1},{4,2},{5,3},{6,4},{7,5},{8,6},{9,7},{10,... | collective-permute-start | bytes 2359304 | tf_op jit(solution)/shard_map/ppermute | solution.py:305
  118.2 34.0 %collective-permute-start.23 = (bf16[3072,128]{1,0:T(8,128)(2,1)}, bf16[3072,128]{1,0:T(8,128)(2,1)}, u32[]{:S(2)}, u32[]{:S(2)}) collective-permute-start(bf16[3072,128]{1,0:T(8,128)(2,1)} %collective-permute-done.21.refs_13_), channel_id=1, source_target_pairs={{0,14},{1,15},{2,0},{3,1},{4,2},{5,3},{6,4},{7,5},{8,6},{9,7},{10,... | collective-permute-start | bytes 2359304 | tf_op jit(solution)/shard_map/ppermute | solution.py:305
  118.3 37.3 %collective-permute-start.16 = (bf16[3072,128]{1,0:T(8,128)(2,1)}, bf16[3072,128]{1,0:T(8,128)(2,1)}, u32[]{:S(2)}, u32[]{:S(2)}) collective-permute-start(bf16[3072,128]{1,0:T(8,128)(2,1)} %collective-permute-done.14.refs_5_), channel_id=1, source_target_pairs={{0,2},{1,3},{2,4},{3,5},{4,6},{5,7},{6,8},{7,9},{8,10},{9,11},{10,... | collective-permute-start | bytes 2359304 | tf_op jit(solution)/shard_map/ppermute | solution.py:305
  136.1 33.6 %collective-permute-start.22 = (bf16[3072,128]{1,0:T(8,128)(2,1)}, bf16[3072,128]{1,0:T(8,128)(2,1)S(1)}, u32[]{:S(2)}, u32[]{:S(2)}) collective-permute-start(bf16[3072,128]{1,0:T(8,128)(2,1)} %collective-permute-done.20.refs_12_), channel_id=1, source_target_pairs={{0,2},{1,3},{2,4},{3,5},{4,6},{5,7},{6,8},{7,9},{8,10},{9,11},{10,... | collective-permute-start | bytes 2359304 | tf_op jit(solution)/shard_map/ppermute | solution.py:305
  136.1 33.6 %collective-permute-start.17 = (bf16[3072,128]{1,0:T(8,128)(2,1)}, bf16[3072,128]{1,0:T(8,128)(2,1)S(1)}, u32[]{:S(2)}, u32[]{:S(2)}) collective-permute-start(bf16[3072,128]{1,0:T(8,128)(2,1)} %collective-permute-done.15.refs_6_), channel_id=1, source_target_pairs={{0,14},{1,15},{2,0},{3,1},{4,2},{5,3},{6,4},{7,5},{8,6},{9,7},{10,... | collective-permute-start | bytes 2359304 | tf_op jit(solution)/shard_map/ppermute | solution.py:305
  152.2 33.7 %collective-permute-start.25 = (bf16[3072,128]{1,0:T(8,128)(2,1)}, bf16[3072,128]{1,0:T(8,128)(2,1)S(1)}, u32[]{:S(2)}, u32[]{:S(2)}) collective-permute-start(bf16[3072,128]{1,0:T(8,128)(2,1)} %collective-permute-done.23.refs_15_), channel_id=1, source_target_pairs={{0,14},{1,15},{2,0},{3,1},{4,2},{5,3},{6,4},{7,5},{8,6},{9,7},{10,... | collective-permute-start | bytes 2359304 | tf_op jit(solution)/shard_map/ppermute | solution.py:305
  155.6 31.0 %collective-permute-start.24 = (bf16[3072,128]{1,0:T(8,128)(2,1)}, bf16[3072,128]{1,0:T(8,128)(2,1)S(1)}, u32[]{:S(2)}, u32[]{:S(2)}) collective-permute-start(bf16[3072,128]{1,0:T(8,128)(2,1)} %collective-permute-done.16.refs_7_), channel_id=1, source_target_pairs={{0,2},{1,3},{2,4},{3,5},{4,6},{5,7},{6,8},{7,9},{8,10},{9,11},{10,... | collective-permute-start | bytes 2359304 | tf_op jit(solution)/shard_map/ppermute | solution.py:305
  155.7 3.4 %collective-permute-start.11 = (bf16[144,2048]{1,0:T(8,128)(2,1)S(1)}, bf16[144,2048]{1,0:T(8,128)(2,1)S(1)}, u32[]{:S(2)}, u32[]{:S(2)}) collective-permute-start(bf16[144,2048]{1,0:T(8,128)(2,1)S(1)} %pad_maximum_fusion.3.refs_0_), channel_id=1, source_target_pairs={{0,1},{1,0},{2,3},{3,2},{4,5},{5,4},{6,7},{7,6},{8,9},{9,8},{10,11... | collective-permute-start | bytes 1769480 | tf_op jit(solution)/shard_map/ppermute | solution.py:310
  192.6 2.4 %collective-permute-start.26 = (bf16[144,2048]{1,0:T(8,128)(2,1)S(1)}, bf16[144,2048]{1,0:T(8,128)(2,1)S(1)}, u32[]{:S(2)}, u32[]{:S(2)}) collective-permute-start(bf16[144,2048]{1,0:T(8,128)(2,1)S(1)} %get-tuple-element.16), channel_id=1, source_target_pairs={{0,1},{1,0},{2,3},{3,2},{4,5},{5,4},{6,7},{7,6},{8,9},{9,8},{10,11... | collective-permute-start | bytes 1769480 | tf_op jit(solution)/shard_map/ppermute | solution.py:310
  195.2 7.6 %copy-start.13 = (f32[64,2]{0,1:T(2,128)S(1)}, f32[64,2]{0,1:T(2,128)}, u32[]{:S(2)}) copy-start(f32[64,2]{0,1:T(2,128)} %param.30) | copy-start | bytes 1540
  196.1 18.2 %copy-start.1 = (f32[64,2048]{1,0:T(8,128)S(1)}, f32[64,2048]{1,0:T(8,128)}, u32[]{:S(2)}) copy-start(f32[64,2048]{1,0:T(8,128)} %copy-done) | copy-start | bytes 1572868
  196.1 18.2 %all-to-all-start.2 = ((bf16[16,144,128]{2,1,0:T(8,128)(2,1)}), bf16[16,144,128]{2,1,0:T(8,128)(2,1)S(1)}, u32[]{:S(2)}, u32[]{:S(2)}) async-start(bf16[16,144,128]{2,1,0:T(8,128)(2,1)} %pad_maximum_fusion.4), calls=%async_computation.2 | async-start | bytes 1179648 | tf_op jit(solution)/shard_map/all_to_all | solution.py:300
